TPU v7x, 256 devices: a whole 4x4x8 slice. The times are simulated.
256 devices in a mesh: sp: 64 (over z, y, core), tp: 4 (over x).
Axes of the slice: x: 4, y: 4, z: 8, core: 2. Of those that a mesh axis runs over, the one named last changes fastest.
Arguments:
- queries: bfloat16 [32768, 1024], P('sp', 'tp'), may hold values from -160 to 160
- keys: bfloat16 [32768, 256], P('sp', 'tp'), may hold values from -5 to 5
- values: bfloat16 [32768, 256], P('sp', 'tp'), may hold values from -6 to 6
- doc_ids: int32 [32768], P('sp'), may hold values from 0 to 31, never falling along the last dimension, each value on 1 to 2048 neighbouring positions
- sink_logit: float32 [16], P('tp'), may hold values from 1 to 6
- w_out: bfloat16 [1024, 2048], P('tp'), may hold values from -0.1875 to 0.1875
- residual: bfloat16 [32768, 2048], P(('sp', 'tp')), may hold values from -6 to 6
- ffn_gain: float32 [2048], replicated, may hold values from 0.1 to 1.9
- expert_ids: int32 [32768, 8], P(('sp', 'tp')), may hold values from 0 to 63, all different within a row; in each aligned block of 64 rows (0 to 63, 64 to 127, ...) at most 12 rows name the same one
- expert_weight: float32 [32768, 8], P(('sp', 'tp')), may hold values from 0.2 to 2
- exp_gate: bfloat16 [64, 2048, 512], P('sp'), may hold values from -0.125 to 0.125
- exp_up: bfloat16 [64, 2048, 512], P('sp'), may hold values from -0.125 to 0.125
- exp_down: bfloat16 [64, 512, 2048], P('sp'), may hold values from -0.25 to 0.25
- shared_gate: bfloat16 [2048, 512], P(None, 'tp'), may hold values from -0.125 to 0.125
- shared_up: bfloat16 [2048, 512], P(None, 'tp'), may hold values from -0.125 to 0.125
- shared_down: bfloat16 [512, 2048], P('tp'), may hold values from -0.25 to 0.25
Outputs:
- output: bfloat16 [32768, 2048], P(('sp', 'tp'))
Inputs may be any that keep to these rules, and one draw needn't show every extreme that they name: `doc_ids`: never falling along the sequence; every document holds at most 2048 positions, and one holds exactly that many. `expert_ids`: each row names 8 different experts. In each aligned block of 64 rows no expert is named by more than 12 rows, and in some blocks one expert is named by exactly 12 rows.
All inputs are finite; a program needn't handle non-finite values.
Results may differ from a plain program's by a relative error of at most 0.018.
Values may be sent and summed in bfloat16 or wider, within the bound.
A program may use at most 128 MiB of HBM per device.

v0:
```python
import jax
import jax.numpy as jnp
from jax import lax
from jax.sharding import PartitionSpec as P

HD = 64
WINDOW = 128


norm_eps = 1e-06


def extended(cells, sides, width):
    for axis, dim in sides:
        count = lax.axis_size(axis)
        ends = count - 1
        head = lax.slice_in_dim(cells, 0, width, axis=dim)
        tail = lax.slice_in_dim(cells, cells.shape[dim] - width, cells.shape[dim], axis=dim)
        cells = jnp.concatenate(
            [
                lax.ppermute(tail, axis, [(i, (i + 1) % count) for i in range(ends)]),
                cells,
                lax.ppermute(head, axis, [((i + 1) % count, i) for i in range(ends)]),
            ],
            axis=dim,
        )
    return cells


def joined_along(blocks, dim):
    blocks = jnp.moveaxis(blocks, 0, dim)
    shape = blocks.shape
    return blocks.reshape(*shape[:dim], shape[dim] * shape[dim + 1], *shape[dim + 2 :])


def piecewise(shard, axis, dim, apply, out_dim):
    devices, rows = (lax.axis_size(axis), shard.shape[dim])
    count = 2 if rows % 2 == 0 else 1
    gathered, length = ([], rows // count)
    for k in range(count):
        share = lax.slice_in_dim(shard, k * length, (k + 1) * length, axis=dim)
        starts = jnp.arange(devices) * rows + k * length
        gathered.append(jax.vmap(apply)(lax.all_gather(share, axis), starts))
    return joined_along(jnp.concatenate(gathered, axis=out_dim + 1), out_dim)


def band_blocks(padded, width):
    span_count = padded.shape[0] // width - 2
    shaped = padded.reshape((span_count + 2, width) + padded.shape[1:])
    return jnp.concatenate(
        [
            shaped[0:span_count:2],
            shaped[1 : span_count + 1 : 2],
            shaped[2 : span_count + 2 : 2],
            shaped[3 : span_count + 3 : 2],
        ],
        axis=1,
    )


def attend(queries, ext_keys, ext_values, ext_marks, own_marks, sink_logit):
    tok_count = queries.shape[0]
    head_count = sink_logit.shape[0]
    key_heads = ext_keys.shape[1] // HD
    group_size = head_count // key_heads
    query_span = 2 * WINDOW
    block_count = tok_count // query_span
    query_blocks = queries.reshape(block_count, query_span, key_heads, group_size, HD)
    key_blocks = band_blocks(ext_keys, WINDOW).reshape(block_count, 4 * WINDOW, key_heads, HD)
    value_blocks = band_blocks(ext_values, WINDOW).reshape(block_count, 4 * WINDOW, key_heads, HD)
    mark_blocks = band_blocks(ext_marks, WINDOW)
    query_marks = own_marks.reshape(block_count, query_span)
    scores = jnp.einsum(
        "nqkgd,nmkd->nkgqm", query_blocks, key_blocks, preferred_element_type=jnp.float32
    ) * HD ** (-0.5)
    offset = (
        jnp.arange(query_span, dtype=jnp.int32)[:, None]
        - jnp.arange(4 * WINDOW, dtype=jnp.int32)[None, :]
        + WINDOW
    )
    allowed = (jnp.abs(offset) <= WINDOW)[None] & (
        mark_blocks[:, None, :] == query_marks[:, :, None]
    )
    scores = jnp.where(allowed[:, None, None], scores, -jnp.inf)
    sink_term = sink_logit.reshape(key_heads, group_size)[None, :, :, None, None]
    row_max = jnp.maximum(jnp.max(scores, axis=-1, keepdims=True), sink_term)
    exp_scores = jnp.exp(scores - row_max)
    attn_probs = (
        exp_scores / (jnp.sum(exp_scores, axis=-1, keepdims=True) + jnp.exp(sink_term - row_max))
    ).astype(jnp.bfloat16)
    result = jnp.einsum(
        "nkgqm,nmkd->nqkgd", attn_probs, value_blocks, preferred_element_type=jnp.float32
    )
    return result.astype(jnp.bfloat16).reshape(tok_count, head_count * HD)


def slot_index(routing, half_rows, slot_cap, expert_count):
    blocks = routing.shape[0] // half_rows
    flat_ids = routing.reshape(blocks, half_rows * routing.shape[1])
    onehot = (
        flat_ids[:, :, None] == jnp.arange(expert_count, dtype=jnp.int32)[None, None, :]
    ).astype(jnp.int32)
    slot_rank = jnp.sum(jnp.cumsum(onehot, axis=1) * onehot, axis=-1) - 1
    slot_place = (
        flat_ids * (blocks * slot_cap)
        + jnp.arange(blocks, dtype=jnp.int32)[:, None] * slot_cap
        + slot_rank
    )
    return slot_place.reshape(-1)


def pack_rows(normed, slot_place, expert_count, per_expert):
    assign_count = slot_place.shape[0]
    top_count = assign_count // normed.shape[0]
    source = (
        jnp.full((expert_count * per_expert,), normed.shape[0], jnp.int32)
        .at[slot_place]
        .set(jnp.arange(assign_count, dtype=jnp.int32) // top_count)
    )
    packed = jnp.take(normed, source, axis=0, mode="fill", fill_value=0)
    return packed.reshape(expert_count, per_expert, normed.shape[1])


def run_expert(arrived, gate_w, up_w, down_w):
    flat_rows = arrived.reshape(-1, arrived.shape[-1])
    hidden = (
        jax.nn.silu(jnp.dot(flat_rows, gate_w, preferred_element_type=jnp.float32))
        * jnp.dot(flat_rows, up_w, preferred_element_type=jnp.float32)
    ).astype(jnp.bfloat16)
    return (
        jnp.dot(hidden, down_w, preferred_element_type=jnp.float32)
        .astype(jnp.bfloat16)
        .reshape(arrived.shape)
    )


def combine_rows(returned, slot_place, weights):
    picked = returned.reshape(-1, returned.shape[-1])[slot_place].reshape(
        weights.shape + (returned.shape[-1],)
    )
    return jnp.sum(weights[:, :, None] * picked.astype(jnp.float32), axis=1)


def shards(
    queries,
    keys,
    values,
    doc_ids,
    sink_logit,
    w_out,
    residual,
    ffn_gain,
    expert_ids,
    expert_weight,
    exp_gate,
    exp_up,
    exp_down,
    shared_gate,
    shared_up,
    shared_down,
):
    marks = (doc_ids + 1).astype(jnp.bfloat16)
    ext_keys, ext_values, ext_marks = (
        extended(keys, (("sp", 0),), WINDOW),
        extended(values, (("sp", 0),), WINDOW),
        extended(marks, (("sp", 0),), WINDOW),
    )
    attended = attend(queries, ext_keys, ext_values, ext_marks, marks, sink_logit)
    row_count = residual.shape[0]
    own_rows = lax.all_to_all(attended, "tp", split_axis=0, concat_axis=1, tiled=True)
    mixed = jnp.dot(
        own_rows,
        lax.all_gather(w_out, "tp", axis=0, tiled=True),
        preferred_element_type=jnp.float32,
    )
    resid = (residual.astype(jnp.float32) + mixed).astype(jnp.bfloat16)
    resid_f = resid.astype(jnp.float32)
    normed = (
        resid_f
        * lax.rsqrt(jnp.mean(resid_f * resid_f, axis=-1, keepdims=True) + norm_eps)
        * ffn_gain
    ).astype(jnp.bfloat16)

    def shared_piece(shard_rows, row_start):
        hidden = (
            jax.nn.silu(jnp.dot(shard_rows, shared_gate, preferred_element_type=jnp.float32))
            * jnp.dot(shard_rows, shared_up, preferred_element_type=jnp.float32)
        ).astype(jnp.bfloat16)
        partial_out = jnp.dot(hidden, shared_down, preferred_element_type=jnp.float32)
        return lax.optimization_barrier(partial_out.astype(jnp.bfloat16)).astype(jnp.float32)

    shared_terms = piecewise(normed, "tp", 0, shared_piece, 0)
    shared_out = lax.psum_scatter(
        shared_terms.astype(jnp.bfloat16), "tp", scatter_dimension=0, tiled=True
    ).astype(jnp.float32)
    expert_count = lax.axis_size("sp") * exp_gate.shape[0]
    top_count = expert_ids.shape[1]
    half_rows = row_count // 2
    slot_cap = min(half_rows, max(2, 3 * half_rows * top_count // (2 * expert_count)))
    slot_place = slot_index(expert_ids, half_rows, slot_cap, expert_count)
    packed = pack_rows(normed, slot_place, expert_count, 2 * slot_cap)
    returned = lax.all_to_all(
        run_expert(
            lax.all_to_all(packed, "sp", split_axis=0, concat_axis=0, tiled=True),
            exp_gate[0],
            exp_up[0],
            exp_down[0],
        ),
        "sp",
        split_axis=0,
        concat_axis=0,
        tiled=True,
    )
    routed = combine_rows(returned, slot_place, expert_weight)
    return (resid.astype(jnp.float32) + shared_out + routed).astype(jnp.bfloat16)


def solution(mesh):
    placed = (
        P("sp", "tp"),
        P("sp", "tp"),
        P("sp", "tp"),
        P("sp"),
        P("tp"),
        P("tp", None),
        P(("sp", "tp"), None),
        P(),
        P(("sp", "tp"), None),
        P(("sp", "tp"), None),
        P("sp", None, None),
        P("sp", None, None),
        P("sp", None, None),
        P(None, "tp"),
        P(None, "tp"),
        P("tp", None),
    )
    return jax.shard_map(
        shards, mesh=mesh, in_specs=placed, out_specs=P(("sp", "tp"), None), check_vma=False
    )
```

profile of v0, /device:TPU:1, one launch (start us, length us, event | category | flops | bytes accessed | tf_op | source)
XLA Modules:
  0.0 426.1 jit_solution(5765054399894328366)
XLA Ops:
  8.0 4.6 %collective-permute-start.2 = (bf16[128]{0:T(256)(128)(2,1)S(1)}, bf16[128]{0:T(256)(128)(2,1)S(1)}, u32[]{:S(2)}, u32[]{:S(2)}) collective-permute-start(bf16[128]{0:T(256)(128)(2,1)S(1)} %get-tuple-element.11), channel_id=1, source_target_pairs={{0,4},{4,8},{8,12},{12,16},{16,20},{20,24},{24,28},{28,32},{32,36}... | collective-permute-start | bytes 776 | tf_op jit(solution)/shard_map/ppermute | solution.py:21
  15.2 3.6 collective-permute-start.4
  21.5 3.6 collective-permute-start
  26.2 2.4 reduce-window.6
  30.1 4.3 %scatter_custom_fusion = s32[1536]{0:T(1024)S(1)} fusion(s32[1024]{0:T(1024)S(1)} %bitcast.133, s32[1024]{0:T(1024)S(1)} %add_select_fusion, s32[]{:T(128)} %constant.28.clone.1), kind=kCustom, calls=%fused_computation.95 | custom fusion | bytes 6148 | tf_op jit(solution)/shard_map/scatter | solution.py:118
  47.8 4.0 all-to-all-start
  51.9 9.2 %all-to-all-done = bf16[4,128,256]{1,2,0:T(8,128)(2,1)S(1)} async-done(((bf16[4,128,256]{1,2,0:T(8,128)(2,1)}), bf16[4,128,256]{1,2,0:T(8,128)(2,1)S(1)}, u32[]{:S(2)}, u32[]{:S(2)}) %all-to-all-start) | async-done | bytes 262176 | tf_op jit(solution)/shard_map/all_to_all | solution.py:170
  61.1 5.3 %all-gather.6.cloned.1.call-done = bf16[1024,2048]{1,0:T(8,128)(2,1)} async-done(((bf16[256,2048]{1,0:T(8,128)(2,1)}), bf16[1024,2048]{1,0:T(8,128)(2,1)}) %all-gather.6.cloned.1.call-update) | async-done | bytes 4194320 | tf_op jit(solution)/shard_map/all_gather | solution.py:173
  66.3 3.0 multiply_reduce_fusion
  70.5 7.0 %gather_fusion = bf16[1536,2048]{1,0:T(8,128)(2,1)} fusion(bf16[128,2048]{1,0:T(8,128)(2,1)S(1)} %multiply_convert_fusion, s32[2048]{0:T(1024)S(1)} %pad_clamp_fusion), kind=kCustom, calls=%fused_computation | custom fusion | bytes 12589056 | tf_op jit(solution)/shard_map/jit(_take)/gather | solution.py:120
  77.6 3.3 broadcast_select_fusion
  80.9 150.4 %all_to_all.29 = bf16[64,24,2048]{2,1,0:T(8,128)(2,1)S(1)} all-to-all(bf16[64,24,2048]{2,1,0:T(8,128)(2,1)S(1)} %broadcast_select_fusion), channel_id=1, replica_groups=mesh['sp'=64,'tp'=4] {'sp'}, dimensions={0} | all-to-all | bytes 12582912 | tf_op jit(solution)/shard_map/all_to_all | solution.py:204
  231.2 2.7 copy-done.4
  234.0 5.1 %fusion.8 = f32[1536,512]{1,0:T(8,128)} fusion(bf16[1536,2048]{1,0:T(8,128)(2,1)S(1)} %bitcast.126, bf16[1,2048,512]{2,1,0:T(8,128)(2,1)S(1)} %copy-done.14), kind=kOutput, calls=%fused_computation.22 | convolution fusion | flops 3221225472 | bytes 11534336 | tf_op jit(solution)/shard_map/dot_general | solution.py:127
  239.1 11.8 %convolution_convert_fusion = bf16[1536,2048]{1,0:T(8,128)(2,1)} fusion(bf16[1,512,2048]{2,1,0:T(8,128)(2,1)S(1)} %copy-done, bf16[1536,2048]{1,0:T(8,128)(2,1)} %bitcast.127, f32[1536,512]{1,0:T(8,128)} %fusion.8, bf16[1,2048,512]{2,1,0:T(8,128)(2,1)} %param.27), kind=kOutput, calls=%fused_computation.5 | convolution fusion | flops 6450315264 | bytes 19922944 | tf_op jit(solution)/shard_map/dot_general | solution.py:131
  250.9 7.3 %all-to-all-start.2 = ((bf16[64,24,2048]{2,1,0:T(8,128)(2,1)}), bf16[64,24,2048]{2,1,0:T(8,128)(2,1)}, u32[]{:S(2)}, u32[]{:S(2)}) async-start(bf16[64,24,2048]{2,1,0:T(8,128)(2,1)} %bitcast.125), calls=%async_computation.3 | async-start | bytes 12582912 | tf_op jit(solution)/shard_map/all_to_all | solution.py:202
  260.1 25.5 %all-gather.8.cloned.1.call-done = bf16[256,2048]{1,0:T(8,128)(2,1)} async-done(((bf16[64,2048]{1,0:T(8,128)(2,1)}), bf16[256,2048]{1,0:T(8,128)(2,1)}) %all-gather.8.cloned.1.call-update) | async-done | bytes 1048592 | tf_op jit(solution)/shard_map/all_gather | solution.py:43
  287.3 2.0 convolution_convert_fusion.2
  289.3 25.3 %all-gather.10.cloned.1.call-done = bf16[256,2048]{1,0:T(8,128)(2,1)} async-done(((bf16[64,2048]{1,0:T(8,128)(2,1)}), bf16[256,2048]{1,0:T(8,128)(2,1)}) %all-gather.10.cloned.1.call-update) | async-done | bytes 1048592 | tf_op jit(solution)/shard_map/all_gather | solution.py:43
  316.3 2.1 convolution_convert_fusion.1
  320.2 77.0 %all-to-all-done.2 = bf16[64,24,2048]{2,1,0:T(8,128)(2,1)} async-done(((bf16[64,24,2048]{2,1,0:T(8,128)(2,1)}), bf16[64,24,2048]{2,1,0:T(8,128)(2,1)}, u32[]{:S(2)}, u32[]{:S(2)}) %all-to-all-start.2) | async-done | bytes 6291488 | tf_op jit(solution)/shard_map/all_to_all | solution.py:202
  397.1 12.6 %gather_fusion.1 = bf16[1024,2048]{1,0:T(8,128)(2,1)} fusion(bf16[1536,2048]{1,0:T(8,128)(2,1)} %bitcast.26, s32[1024]{0:T(1024)S(1)} %broadcast_clamp_fusion), kind=kCustom, calls=%fused_computation.1 | custom fusion | bytes 8392704 | tf_op jit(solution)/shard_map/gather | solution.py:138
  409.7 7.6 %fusion = f32[128,2048]{1,0:T(8,128)} fusion(bf16[1024,2048]{1,0:T(8,128)(2,1)} %gather_fusion.1, f32[128,8]{1,0:T(8,128)S(1)} %copy.51), kind=kLoop, calls=%fused_computation.4 | loop fusion | flops 6029312 | bytes 5246976 | tf_op jit(solution)/shard_map/reduce_sum | solution.py:141
  417.3 2.3 add_convert_fusion
  (119 shorter events, 30.4 us)
Async XLA Ops:
  6.5 232.6 %copy-start = (bf16[1,512,2048]{2,1,0:T(8,128)(2,1)S(1)}, bf16[1,512,2048]{2,1,0:T(8,128)(2,1)}, u32[]{:S(2)}) copy-start(bf16[1,512,2048]{2,1,0:T(8,128)(2,1)} %param.28) | copy-start | bytes 6291460
  6.5 31.7 %copy-start.9 = (bf16[512,64]{0,1:T(8,128)(2,1)S(1)}, bf16[512,64]{0,1:T(8,128)(2,1)}, u32[]{:S(2)}) copy-start(bf16[512,64]{0,1:T(8,128)(2,1)} %param.17) | copy-start | bytes 196612
  6.5 34.8 %copy-start.10 = (bf16[512,64]{0,1:T(8,128)(2,1)S(1)}, bf16[512,64]{0,1:T(8,128)(2,1)}, u32[]{:S(2)}) copy-start(bf16[512,64]{0,1:T(8,128)(2,1)} %param.18) | copy-start | bytes 196612
  6.5 59.8 %all-gather.6.cloned.1.call-start = ((), (), s32[]{:S(2)}) async-start(), calls=%async_computation.4 | async-start | bytes 5242880 | tf_op jit(solution)/shard_map/all_gather | solution.py:173
  8.0 27.9 %collective-permute-start.2 = (bf16[128]{0:T(256)(128)(2,1)S(1)}, bf16[128]{0:T(256)(128)(2,1)S(1)}, u32[]{:S(2)}, u32[]{:S(2)}) collective-permute-start(bf16[128]{0:T(256)(128)(2,1)S(1)} %get-tuple-element.11), channel_id=1, source_target_pairs={{0,4},{4,8},{8,12},{12,16},{16,20},{20,24},{24,28},{28,32},{32,36}... | collective-permute-start | bytes 776 | tf_op jit(solution)/shard_map/ppermute | solution.py:21
  12.5 25.3 %collective-permute-start.3 = (bf16[128]{0:T(256)(128)(2,1)S(1)}, bf16[128]{0:T(256)(128)(2,1)S(1)}, u32[]{:S(2)}, u32[]{:S(2)}) collective-permute-start(bf16[128]{0:T(256)(128)(2,1)S(1)} %get-tuple-element.12), channel_id=1, source_target_pairs={{4,0},{8,4},{12,8},{16,12},{20,16},{24,20},{28,24},{32,28},{36,32}... | collective-permute-start | bytes 776 | tf_op jit(solution)/shard_map/ppermute | solution.py:23
  15.2 23.0 %collective-permute-start.4 = (bf16[128,64]{0,1:T(8,128)(2,1)S(1)}, bf16[128,64]{0,1:T(8,128)(2,1)S(1)}, u32[]{:S(2)}, u32[]{:S(2)}) collective-permute-start(bf16[128,64]{0,1:T(8,128)(2,1)S(1)} %get-tuple-element.9), channel_id=1, source_target_pairs={{0,4},{4,8},{8,12},{12,16},{16,20},{20,24},{24,28},{28,32},{32,36}... | collective-permute-start | bytes 49160 | tf_op jit(solution)/shard_map/ppermute | solution.py:21
  18.8 19.4 %collective-permute-start.5 = (bf16[128,64]{0,1:T(8,128)(2,1)S(1)}, bf16[128,64]{0,1:T(8,128)(2,1)S(1)}, u32[]{:S(2)}, u32[]{:S(2)}) collective-permute-start(bf16[128,64]{0,1:T(8,128)(2,1)S(1)} %get-tuple-element.10), channel_id=1, source_target_pairs={{4,0},{8,4},{12,8},{16,12},{20,16},{24,20},{28,24},{32,28},{36,32}... | collective-permute-start | bytes 49160 | tf_op jit(solution)/shard_map/ppermute | solution.py:23
  21.5 18.6 %collective-permute-start = (bf16[128,64]{0,1:T(8,128)(2,1)S(1)}, bf16[128,64]{0,1:T(8,128)(2,1)S(1)}, u32[]{:S(2)}, u32[]{:S(2)}) collective-permute-start(bf16[128,64]{0,1:T(8,128)(2,1)S(1)} %get-tuple-element.7), channel_id=1, source_target_pairs={{0,4},{4,8},{8,12},{12,16},{16,20},{20,24},{24,28},{28,32},{32,36}... | collective-permute-start | bytes 49160 | tf_op jit(solution)/shard_map/ppermute | solution.py:21
  34.6 9.6 %copy-start.13 = (f32[4]{0:T(128)S(1)}, f32[4]{0:T(128)}, u32[]{:S(2)}) copy-start(f32[4]{0:T(128)} %param.20) | copy-start | bytes 52
  35.9 5.5 %collective-permute-start.1 = (bf16[128,64]{0,1:T(8,128)(2,1)S(1)}, bf16[128,64]{0,1:T(8,128)(2,1)S(1)}, u32[]{:S(2)}, u32[]{:S(2)}) collective-permute-start(bf16[128,64]{0,1:T(8,128)(2,1)S(1)} %get-tuple-element.8), channel_id=1, source_target_pairs={{4,0},{8,4},{12,8},{16,12},{20,16},{24,20},{28,24},{32,28},{36,32}... | collective-permute-start | bytes 49160 | tf_op jit(solution)/shard_map/ppermute | solution.py:23
  45.3 21.1 %copy-start.8 = (bf16[128,2048]{1,0:T(8,128)(2,1)S(1)}, bf16[128,2048]{1,0:T(8,128)(2,1)}, u32[]{:S(2)}) copy-start(bf16[128,2048]{1,0:T(8,128)(2,1)} %param.22) | copy-start | bytes 1572868
  46.5 23.8 %copy-start.11 = (f32[2048]{0:T(1024)S(1)}, f32[2048]{0:T(1024)}, u32[]{:S(2)}) copy-start(f32[2048]{0:T(1024)} %param.23) | copy-start | bytes 24580
  47.8 13.3 %all-to-all-start = ((bf16[4,128,256]{1,2,0:T(8,128)(2,1)}), bf16[4,128,256]{1,2,0:T(8,128)(2,1)S(1)}, u32[]{:S(2)}, u32[]{:S(2)}) async-start(bf16[4,128,256]{1,2,0:T(8,128)(2,1)} %copy.50), calls=%async_computation | async-start | bytes 524288 | tf_op jit(solution)/shard_map/all_to_all | solution.py:170
  80.8 153.1 %copy-start.14 = (bf16[1,2048,512]{2,1,0:T(8,128)(2,1)S(1)}, bf16[1,2048,512]{2,1,0:T(8,128)(2,1)}, u32[]{:S(2)}) copy-start(bf16[1,2048,512]{2,1,0:T(8,128)(2,1)} %param.26) | copy-start | bytes 6291460
  250.9 34.8 %copy-start.7 = (bf16[2048,128]{1,0:T(8,128)(2,1)S(1)}, bf16[2048,128]{1,0:T(8,128)(2,1)}, u32[]{:S(2)}) copy-start(bf16[2048,128]{1,0:T(8,128)(2,1)} %param.29) | copy-start | bytes 1572868
  250.9 36.4 %copy-start.5 = (bf16[128,2048]{1,0:T(8,128)(2,1)S(1)}, bf16[128,2048]{1,0:T(8,128)(2,1)}, u32[]{:S(2)}) copy-start(bf16[128,2048]{1,0:T(8,128)(2,1)} %param.31) | copy-start | bytes 1572868
  250.9 36.4 %copy-start.6 = (bf16[2048,128]{1,0:T(8,128)(2,1)S(1)}, bf16[2048,128]{1,0:T(8,128)(2,1)}, u32[]{:S(2)}) copy-start(bf16[2048,128]{1,0:T(8,128)(2,1)} %param.30) | copy-start | bytes 1572868
  250.9 146.2 %all-to-all-start.2 = ((bf16[64,24,2048]{2,1,0:T(8,128)(2,1)}), bf16[64,24,2048]{2,1,0:T(8,128)(2,1)}, u32[]{:S(2)}, u32[]{:S(2)}) async-start(bf16[64,24,2048]{2,1,0:T(8,128)(2,1)} %bitcast.125), calls=%async_computation.3 | async-start | bytes 12582912 | tf_op jit(solution)/shard_map/all_to_all | solution.py:202
  258.2 27.4 %all-gather.8.cloned.1.call-start = ((), (), s32[]{:S(2)}) async-start(), calls=%async_computation.6 | async-start | bytes 1310720 | tf_op jit(solution)/shard_map/all_gather | solution.py:43
  259.1 55.5 %all-gather.10.cloned.1.call-start = ((), (), s32[]{:S(2)}) async-start(), calls=%async_computation.7 | async-start | bytes 1310720 | tf_op jit(solution)/shard_map/all_gather | solution.py:43
  259.9 157.4 %reduce-scatter.2.cloned.1.call-start = ((), (), s32[]{:S(2)}) async-start(), calls=%async_computation.5 | async-start | bytes 2621440 | tf_op jit(solution)/shard_map/reduce_scatter | solution.py:193
  397.1 22.5 %copy-start.1 = (bf16[1,512,2048]{2,1,0:T(8,128)(2,1)S(1)}, bf16[1,512,2048]{2,1,0:T(8,128)(2,1)}, u32[]{:S(2)}) copy-start(bf16[1,512,2048]{2,1,0:T(8,128)(2,1)} %param.28) | copy-start | bytes 6291460
  409.7 7.6 %copy-start.3 = (f32[128,2048]{1,0:T(8,128)S(1)}, f32[128,2048]{1,0:T(8,128)}, u32[]{:S(2)}) copy-start(f32[128,2048]{1,0:T(8,128)} %copy-done.2) | copy-start | bytes 3145732
  (3 other events, 7.5 us)
Sparse Core Ops, SparseCore 0:
  9.1 57.1 all-gather.5
  260.9 24.7 all-gather.7
  287.5 27.1 all-gather.9
  320.2 34.3 reduce-scatter.1
where the time goes:
time: 428 us; the launch traced here: 426 us
  blocking collectives  150 us (35%)
  waiting for transfers between devices  145 us (34%)
  local copies, waits for them, and re-layouts  37.9 us (9%)
  matrix products  29.5 us (7%)
  starting transfers between devices  29.3 us (7%)
  other arithmetic  20.4 us (5%)
  between operations  13.6 us (3%)
    all_to_all x1, blocking collectives, shards(): lax.all_to_all(packed, 'sp', split_axis=0, concat_axis=0, tiled=True)  150 us
    all_to_all x1, waiting for transfers between devices, shards(): lax.all_to_all(run_expert(lax.all_to_all(packed, 'sp', split_axis=0, conc...  77 us
    all_gather x2, waiting for transfers between devices, piecewise(): gathered.append(jax.vmap(apply)(lax.all_gather(share, axis), starts))  50.8 us
    gather x1, local copies, waits for them, and re-layouts, combine_rows(): returned.reshape(-1, returned.shape[-1])[slot_place]  12.6 us
    ppermute x3, starting transfers between devices, extended(): lax.ppermute(tail, axis, [(i, (i + 1) % count) for i in range(ends)])  11.8 us
    dot_general x1, matrix products, run_expert(): jnp.dot(hidden, down_w, preferred_element_type=jnp.float32)  11.8 us
    all_to_all x1, waiting for transfers between devices, shards(): lax.all_to_all(attended, 'tp', split_axis=0, concat_axis=1, tiled=True)  9.17 us
  transfers between devices with their start and end apart: 12, of which 6 were waited for; matrix products, arithmetic and copies ran while one was open for 12% of the time, Pallas kernels for 0%

commit v1 on v0

v1 whole, which is shorter than its diff:
```python
import functools

import jax
import jax.numpy as jnp
from jax import lax
from jax.experimental import pallas as pl
from jax.experimental.pallas import tpu as pltpu
from jax.sharding import PartitionSpec as P

HD = 64
WINDOW = 128
NZ, NY, NC, NX = 8, 4, 2, 4
PLANE = NY * NC
ROWS = 128
HALF = 64
CAP = 12
SLOTS = 2 * CAP
PACK = PLANE * SLOTS
D = 2048
FF = 512
EXPERTS = 64
MESH = pl.DeviceIdType.MESH
BF = jnp.bfloat16
F32 = jnp.float32

norm_eps = 1e-06


def extended(cells, sides, width):
    for axis, dim in sides:
        count = lax.axis_size(axis)
        ends = count - 1
        head = lax.slice_in_dim(cells, 0, width, axis=dim)
        tail = lax.slice_in_dim(cells, cells.shape[dim] - width, cells.shape[dim], axis=dim)
        cells = jnp.concatenate(
            [
                lax.ppermute(tail, axis, [(i, (i + 1) % count) for i in range(ends)]),
                cells,
                lax.ppermute(head, axis, [((i + 1) % count, i) for i in range(ends)]),
            ],
            axis=dim,
        )
    return cells


def band_blocks(padded, width):
    span_count = padded.shape[0] // width - 2
    shaped = padded.reshape((span_count + 2, width) + padded.shape[1:])
    return jnp.concatenate(
        [
            shaped[0:span_count:2],
            shaped[1 : span_count + 1 : 2],
            shaped[2 : span_count + 2 : 2],
            shaped[3 : span_count + 3 : 2],
        ],
        axis=1,
    )


def attend(queries, ext_keys, ext_values, ext_marks, own_marks, sink_logit):
    tok_count = queries.shape[0]
    head_count = sink_logit.shape[0]
    key_heads = ext_keys.shape[1] // HD
    group_size = head_count // key_heads
    query_span = 2 * WINDOW
    block_count = tok_count // query_span
    query_blocks = queries.reshape(block_count, query_span, key_heads, group_size, HD)
    key_blocks = band_blocks(ext_keys, WINDOW).reshape(block_count, 4 * WINDOW, key_heads, HD)
    value_blocks = band_blocks(ext_values, WINDOW).reshape(block_count, 4 * WINDOW, key_heads, HD)
    mark_blocks = band_blocks(ext_marks, WINDOW)
    query_marks = own_marks.reshape(block_count, query_span)
    scores = jnp.einsum(
        "nqkgd,nmkd->nkgqm", query_blocks, key_blocks, preferred_element_type=jnp.float32
    ) * HD ** (-0.5)
    offset = (
        jnp.arange(query_span, dtype=jnp.int32)[:, None]
        - jnp.arange(4 * WINDOW, dtype=jnp.int32)[None, :]
        + WINDOW
    )
    allowed = (jnp.abs(offset) <= WINDOW)[None] & (
        mark_blocks[:, None, :] == query_marks[:, :, None]
    )
    scores = jnp.where(allowed[:, None, None], scores, -jnp.inf)
    sink_term = sink_logit.reshape(key_heads, group_size)[None, :, :, None, None]
    row_max = jnp.maximum(jnp.max(scores, axis=-1, keepdims=True), sink_term)
    exp_scores = jnp.exp(scores - row_max)
    attn_probs = (
        exp_scores / (jnp.sum(exp_scores, axis=-1, keepdims=True) + jnp.exp(sink_term - row_max))
    ).astype(jnp.bfloat16)
    result = jnp.einsum(
        "nkgqm,nmkd->nqkgd", attn_probs, value_blocks, preferred_element_type=jnp.float32
    )
    return result.astype(jnp.bfloat16).reshape(tok_count, head_count * HD)


def dot(a, b):
    return jnp.dot(a, b, preferred_element_type=F32)


def silu(v):
    return v / (1.0 + jnp.exp(-v))


def chunk_of(delta):
    return 0 if delta == 0 else (2 * delta - 1 if delta <= NZ // 2 else 2 * (NZ - delta))


def moe_kernel(
    normed, resid, ids, weight, eg, eu, ed, shg, shu, shd, out,
    tok, tx, rx, eo, ret, rst, rsx, info, inf, wg, wu, wd, sg, su, sd, sacc, hid,
    z_s, z_r, i_s, i_r, d_s, d_r, e_s, e_r, p_s, p_r, x_s, x_r, w_s,
):
    sp, x = lax.axis_index("sp"), lax.axis_index("tp")
    z, mine = sp // PLANE, sp % PLANE

    def at_z(dz):
        return ((z + dz) % NZ * PLANE + mine, x)

    def at_plane(j):
        return (z * PLANE + j, x)

    def at_x(dx):
        return (sp, (x + dx) % NX)

    def send(src, dst, ssem, rsem, device):
        copy = pltpu.make_async_remote_copy(
            src_ref=src, dst_ref=dst, send_sem=ssem, recv_sem=rsem, device_id=device, device_id_type=MESH
        )
        copy.start()

    def landed(ref, sem):
        pltpu.make_async_copy(ref, ref, sem).wait()

    local = [
        pltpu.make_async_copy(normed, tok.at[0], w_s.at[0]),
        pltpu.make_async_copy(shg, sg.at[0], w_s.at[1]),
        pltpu.make_async_copy(shu, su.at[0], w_s.at[2]),
        pltpu.make_async_copy(shd, sd.at[0], w_s.at[3]),
        pltpu.make_async_copy(eg.at[0], wg, w_s.at[4]),
        pltpu.make_async_copy(eu.at[0], wu, w_s.at[5]),
        pltpu.make_async_copy(ed.at[0], wd, w_s.at[6]),
    ]
    for copy in local:
        copy.start()

    barrier = pltpu.get_barrier_semaphore()
    peers = [at_z(dz) for dz in range(1, NZ)] + [at_x(dx) for dx in range(1, NX)]
    peers += [at_plane((mine + off) % PLANE) for off in range(1, PLANE)]
    for device in peers:
        pl.semaphore_signal(barrier, inc=1, device_id=device, device_id_type=MESH)

    expert = lax.broadcasted_iota(jnp.int32, (EXPERTS, ROWS), 0)
    hits = jnp.zeros((EXPERTS, ROWS), F32)
    wide = jnp.zeros((EXPERTS, ROWS), F32)
    for k in range(ids.shape[0]):
        named = ids[k : k + 1, :] == expert
        hits = hits + named.astype(F32)
        wide = wide + jnp.where(named, weight[k : k + 1, :], 0.0)
    row = lax.broadcasted_iota(jnp.int32, (ROWS, ROWS), 0)
    col = lax.broadcasted_iota(jnp.int32, (ROWS, ROWS), 1)
    earlier = ((row < col) & (row // HALF == col // HALF)).astype(BF)
    rank = dot(hits.astype(BF), earlier)
    half = lax.broadcasted_iota(jnp.int32, (EXPERTS, ROWS), 1) // HALF
    place = jnp.where(hits > 0.0, rank + (half * CAP).astype(F32), -1.0)
    for plane in range(NZ):
        lower = plane * PLANE
        info[plane, 0:PLANE, :] = place[lower : lower + PLANE]
        info[plane, PLANE : 2 * PLANE, :] = wide[lower : lower + PLANE]
    inf[0] = info[z]

    local[0].wait()
    pl.semaphore_wait(barrier, len(peers))
    for delta in range(1, NZ):
        i = chunk_of(delta)
        send(info.at[(z + delta) % NZ], inf.at[i], i_s.at[i], i_r.at[i], at_z(delta))
    send(tok.at[0], tok.at[1], z_s.at[1], z_r.at[1], at_z(1))
    send(tok.at[0], tok.at[2], z_s.at[2], z_r.at[2], at_z(NZ - 1))

    def placed(i):
        slot = lax.broadcasted_iota(jnp.int32, (PLANE, SLOTS, ROWS), 1).astype(F32)
        return (inf[i, 0:PLANE, :][:, None, :] == slot).astype(F32)

    def dispatch(i):
        @pl.when(i > 0)
        def _():
            landed(tok.at[i], z_r.at[i])
            landed(inf.at[i], i_r.at[i])

        @pl.when((i > 0) & (i + 2 < NZ))
        def _():
            way = 1 + (NZ - 2) * ((i + 1) % 2)
            send(tok.at[i], tok.at[i + 2], z_s.at[i + 2], z_r.at[i + 2], at_z(way))

        pick = placed(i).reshape(PACK, ROWS).astype(BF)
        for n in range(D // 512):
            cols = pl.ds(n * 512, 512)
            tx[i, :, :, cols] = dot(pick, tok[i, :, cols]).astype(BF).reshape(PLANE, SLOTS, 512)
        for off in range(1, PLANE):
            j = (mine + off) % PLANE
            send(tx.at[i, j], rx.at[i, mine], d_s.at[i], d_r.at[i], at_plane(j))
        pltpu.make_async_copy(tx.at[i, mine], rx.at[i, mine], d_r.at[i]).start()

    def run_expert(i):
        landed(rx.at[i], d_r.at[i])

        def hidden_tile(n, carry):
            cols = pl.ds(pl.multiple_of(n * 256, 256), 256)
            rows = rx[i].reshape(PACK, D)
            hid[:, cols] = (silu(dot(rows, wg[:, cols])) * dot(rows, wu[:, cols])).astype(BF)
            return carry

        lax.fori_loop(0, FF // 256, hidden_tile, 0)

        def out_tile(n, carry):
            cols = pl.ds(pl.multiple_of(n * 512, 512), 512)
            eo[i, :, :, cols] = dot(hid[...], wd[:, cols]).astype(BF).reshape(PLANE, SLOTS, 512)
            return carry

        lax.fori_loop(0, D // 512, out_tile, 0)

    def give_back(i):
        for off in range(1, PLANE):
            j = (mine + off) % PLANE
            send(eo.at[i, j], ret.at[i, mine], e_s.at[i], e_r.at[i], at_plane(j))
        pltpu.make_async_copy(eo.at[i, mine], ret.at[i, mine], e_r.at[i]).start()

    LAG = 2

    def forward(i, carry):
        @pl.when(i < NZ)
        def _():
            dispatch(i)

        @pl.when(i == 0)
        def _():
            for dx in range(1, NX):
                send(sg.at[0], sg.at[dx], x_s.at[0, dx], x_r.at[0, dx], at_x(dx))
                send(su.at[0], su.at[dx], x_s.at[1, dx], x_r.at[1, dx], at_x(dx))
                send(sd.at[0], sd.at[dx], x_s.at[2, dx], x_r.at[2, dx], at_x(dx))

        @pl.when(i >= LAG)
        def _():
            run_expert(i - LAG)

        @pl.when(i >= NZ - 2 + LAG)
        def _():
            give_back(i - LAG)

        return carry

    for copy in local[1:]:
        copy.wait()
    lax.fori_loop(0, NZ + LAG, forward, 0)

    def backward(n, carry):
        give_back(NZ - 3 - n)
        return carry

    lax.fori_loop(0, NZ - 2, backward, 0)

    for dx in range(1, NX):
        landed(sg.at[dx], x_r.at[0, dx])
        landed(su.at[dx], x_r.at[1, dx])
        landed(sd.at[dx], x_r.at[2, dx])
    sacc[...] = jnp.zeros_like(sacc)

    def shared_block(dx, carry):
        rows = tok[0]
        units = (silu(dot(rows, sg[dx])) * dot(rows, su[dx])).astype(BF)
        for n in range(D // 512):
            cols = pl.ds(n * 512, 512)
            sacc[:, cols] = sacc[:, cols] + dot(units, sd[dx, :, cols])
        return carry

    lax.fori_loop(0, NX, shared_block, 0)

    def combined(i):
        landed(ret.at[i], e_r.at[i])
        scaled = placed(i) * inf[i, PLANE : 2 * PLANE, :][:, None, :]
        scaled = jnp.concatenate([scaled.reshape(PACK, ROWS), jnp.zeros((256 - PACK, ROWS), F32)], axis=0)
        scaled = scaled.T[:, :PACK]
        high = scaled.astype(BF)
        low = (scaled - high.astype(F32)).astype(BF)

        def part(cols):
            rows = ret[i, :, :, cols].reshape(PACK, 512)
            return dot(high, rows) + dot(low, rows)

        return part

    def pass_on(i):
        way = NZ - 1 - (NZ - 2) * ((i + 1) % 2)
        send(rst.at[i], rsx.at[i], p_s.at[i], p_r.at[i], at_z(way))

    def farthest(n, carry):
        i = NZ - 1 - n
        part = combined(i)
        for n in range(D // 512):
            cols = pl.ds(n * 512, 512)
            rst[i, :, cols] = part(cols).astype(BF)
        pass_on(i)
        return carry

    lax.fori_loop(0, 2, farthest, 0)

    def nearer(n, carry):
        i = NZ - 3 - n
        part = combined(i)
        landed(rsx.at[i + 2], p_r.at[i + 2])
        for n in range(D // 512):
            cols = pl.ds(n * 512, 512)
            rst[i, :, cols] = (part(cols) + rsx[i + 2, :, cols].astype(F32)).astype(BF)
        pass_on(i)
        return carry

    lax.fori_loop(0, NZ - 3, nearer, 0)

    part = combined(0)
    landed(rsx.at[2], p_r.at[2])
    landed(rsx.at[1], p_r.at[1])
    for n in range(D // 512):
        cols = pl.ds(n * 512, 512)
        routed = part(cols) + rsx[2, :, cols].astype(F32) + rsx[1, :, cols].astype(F32)
        out[:, cols] = (resid[:, cols].astype(F32) + sacc[:, cols] + routed).astype(BF)

    for i in range(NZ):
        landed(tx.at[i, pl.ds(0, PLANE - 1)], d_s.at[i])
        landed(eo.at[i, pl.ds(0, PLANE - 1)], e_s.at[i])
        if i > 0:
            landed(tok.at[i], z_s.at[i])
            landed(info.at[i], i_s.at[i])
            landed(rst.at[i], p_s.at[i])
    for dx in range(1, NX):
        landed(sg.at[0], x_s.at[0, dx])
        landed(su.at[0], x_s.at[1, dx])
        landed(sd.at[0], x_s.at[2, dx])


def moe(normed, resid, ids, weight, eg, eu, ed, shg, shu, shd):
    vmem = pl.BlockSpec(memory_space=pltpu.VMEM)
    hbm = pl.BlockSpec(memory_space=pl.ANY)
    dma = pltpu.SemaphoreType.DMA
    unit = FF // NX
    return pl.pallas_call(
        moe_kernel,
        out_shape=jax.ShapeDtypeStruct((ROWS, D), BF),
        in_specs=[hbm, vmem, vmem, vmem] + [hbm] * 6,
        out_specs=vmem,
        scratch_shapes=[
            pltpu.VMEM((NZ, ROWS, D), BF),
            pltpu.VMEM((NZ, PLANE, SLOTS, D), BF),
            pltpu.VMEM((NZ, PLANE, SLOTS, D), BF),
            pltpu.VMEM((NZ, PLANE, SLOTS, D), BF),
            pltpu.VMEM((NZ, PLANE, SLOTS, D), BF),
            pltpu.VMEM((NZ, ROWS, D), BF),
            pltpu.VMEM((NZ, ROWS, D), BF),
            pltpu.VMEM((NZ, 2 * PLANE, ROWS), F32),
            pltpu.VMEM((NZ, 2 * PLANE, ROWS), F32),
            pltpu.VMEM((D, FF), BF),
            pltpu.VMEM((D, FF), BF),
            pltpu.VMEM((FF, D), BF),
            pltpu.VMEM((NX, D, unit), BF),
            pltpu.VMEM((NX, D, unit), BF),
            pltpu.VMEM((NX, unit, D), BF),
            pltpu.VMEM((ROWS, D), F32),
            pltpu.VMEM((PACK, FF), BF),
        ]
        + [dma((NZ,))] * 10
        + [dma((3, NX)), dma((3, NX)), dma((7,))],
        compiler_params=pltpu.CompilerParams(
            collective_id=1, has_side_effects=True, vmem_limit_bytes=62 * 2**20
        ),
        name="moe",
    )(normed, resid, ids, weight, eg, eu, ed, shg, shu, shd)


def shards(
    queries,
    keys,
    values,
    doc_ids,
    sink_logit,
    w_out,
    residual,
    ffn_gain,
    expert_ids,
    expert_weight,
    exp_gate,
    exp_up,
    exp_down,
    shared_gate,
    shared_up,
    shared_down,
):
    marks = (doc_ids + 1).astype(jnp.bfloat16)
    ext_keys, ext_values, ext_marks = (
        extended(keys, (("sp", 0),), WINDOW),
        extended(values, (("sp", 0),), WINDOW),
        extended(marks, (("sp", 0),), WINDOW),
    )
    attended = attend(queries, ext_keys, ext_values, ext_marks, marks, sink_logit)
    own_rows = lax.all_to_all(attended, "tp", split_axis=0, concat_axis=1, tiled=True)
    mixed = jnp.dot(
        own_rows,
        lax.all_gather(w_out, "tp", axis=0, tiled=True),
        preferred_element_type=jnp.float32,
    )
    resid = (residual.astype(jnp.float32) + mixed).astype(jnp.bfloat16)
    resid_f = resid.astype(jnp.float32)
    normed = (
        resid_f
        * lax.rsqrt(jnp.mean(resid_f * resid_f, axis=-1, keepdims=True) + norm_eps)
        * ffn_gain
    ).astype(jnp.bfloat16)
    return moe(
        normed, resid, expert_ids.T, expert_weight.T, exp_gate, exp_up, exp_down,
        shared_gate, shared_up, shared_down,
    )


def solution(mesh):
    placed = (
        P("sp", "tp"),
        P("sp", "tp"),
        P("sp", "tp"),
        P("sp"),
        P("tp"),
        P("tp", None),
        P(("sp", "tp"), None),
        P(),
        P(("sp", "tp"), None),
        P(("sp", "tp"), None),
        P("sp", None, None),
        P("sp", None, None),
        P("sp", None, None),
        P(None, "tp"),
        P(None, "tp"),
        P("tp", None),
    )
    return jax.shard_map(
        shards, mesh=mesh, in_specs=placed, out_specs=P(("sp", "tp"), None), check_vma=False
    )
```

time: 428 us -> 239 us (0.56)
  Pallas kernels: 0 us -> 159 us
  blocking collectives: 150 us -> 13.1 us
  waiting for transfers between devices: 145 us -> 15.8 us
  local copies, waits for them, and re-layouts: 37.9 us -> 8.82 us
  matrix products: 29.5 us -> 5.21 us
  other arithmetic: 20.4 us -> 4.85 us
  starting transfers between devices: 29.3 us -> 17.6 us
    pallas_call x0 -> x1, Pallas kernels: none -> 159 us  [moe(): pl.pallas_call(moe_kernel, out_shape=jax.ShapeDtypeStruct((ROWS, D), BF),...]
    all_to_all x1, blocking collectives: 150 us -> 13.1 us  [shards(): lax.all_to_all(attended, 'tp', split_axis=0, concat_axis=1, tiled=True)]
    all_to_all x2 -> x0, waiting for transfers between devices: 86.1 us -> none  [the longest x1 77 us: shards(): lax.all_to_all(run_expert(lax.all_to_all(packed, 'sp', split_axis=0, conc...]
    all_gather x2 -> x0, waiting for transfers between devices: 50.8 us -> none  [piecewise(): gathered.append(jax.vmap(apply)(lax.all_gather(share, axis), starts))]
    dot_general x6 -> x0, matrix products: 24.3 us -> none  [the longest x1 11.8 us: run_expert(): jnp.dot(hidden, down_w, preferred_element_type=jnp.float32)]
    gather x2 -> x0, local copies, waits for them, and re-layouts: 19.6 us -> none  [the longest x1 12.6 us: combine_rows(): returned.reshape(-1, returned.shape[-1])[slot_place]]
    all_to_all x2 -> x0, starting transfers between devices: 11.3 us -> none  [the longest x1 7.33 us: shards(): lax.all_to_all(run_expert(lax.all_to_all(packed, 'sp', split_axis=0, conc...]
    all_gather x1, waiting for transfers between devices: 5.28 us -> 14.6 us  [shards(): lax.all_gather(w_out, 'tp', axis=0, tiled=True)]
  transfers between devices with their start and end apart: 12 -> 7, of which waited for: 6 -> 2; matrix products, arithmetic and copies ran while one was open for 12% -> 5% of each run, Pallas kernels for 0% -> 0%
where the time goes in v1:
time: 239 us; the launch traced here: 238 us
  Pallas kernels  159 us (67%)
  starting transfers between devices  17.6 us (7%)
  waiting for transfers between devices  15.8 us (7%)
  between operations  13.7 us (6%)
  blocking collectives  13.1 us (5%)
  local copies, waits for them, and re-layouts  8.82 us (4%)
  matrix products  5.21 us (2%)
  other arithmetic  4.85 us (2%)
    pallas_call x1, Pallas kernels, moe(): pl.pallas_call(moe_kernel, out_shape=jax.ShapeDtypeStruct((ROWS, D), BF),...  159 us
    all_gather x1, waiting for transfers between devices, shards(): lax.all_gather(w_out, 'tp', axis=0, tiled=True)  14.6 us
    all_to_all x1, blocking collectives, shards(): lax.all_to_all(attended, 'tp', split_axis=0, concat_axis=1, tiled=True)  13.1 us
    ppermute x3, starting transfers between devices, extended(): lax.ppermute(tail, axis, [(i, (i + 1) % count) for i in range(ends)])  11.8 us
    ppermute x3, starting transfers between devices, extended(): lax.ppermute(head, axis, [((i + 1) % count, i) for i in range(ends)])  5.76 us
  transfers between devices with their start and end apart: 7, of which 2 were waited for; matrix products, arithmetic and copies ran while one was open for 5% of the time, Pallas kernels for 0%

profile of v1, /device:TPU:1, one launch (start us, length us, event | category | flops | bytes accessed | tf_op | source)
XLA Modules:
  0.0 238.0 jit_solution(4108691718044219408)
XLA Ops:
  6.5 0.7 all-gather.2.cloned.1.call-update
  7.3 0.7 add_convert_fusion
  8.0 4.6 %collective-permute-start.2 = (bf16[128]{0:T(256)(128)(2,1)S(1)}, bf16[128]{0:T(256)(128)(2,1)S(1)}, u32[]{:S(2)}, u32[]{:S(2)}) collective-permute-start(bf16[128]{0:T(256)(128)(2,1)S(1)} %get-tuple-element.9), channel_id=1, source_target_pairs={{0,4},{4,8},{8,12},{12,16},{16,20},{20,24},{24,28},{28,32},{32,36}... | collective-permute-start | bytes 776 | tf_op jit(solution)/shard_map/ppermute | solution.py:37
  12.5 1.9 collective-permute-start.3
  14.5 0.7 fusion.33
  15.2 3.6 %collective-permute-start.4 = (bf16[128,64]{0,1:T(8,128)(2,1)S(1)}, bf16[128,64]{0,1:T(8,128)(2,1)S(1)}, u32[]{:S(2)}, u32[]{:S(2)}) collective-permute-start(bf16[128,64]{0,1:T(8,128)(2,1)S(1)} %get-tuple-element.7), channel_id=1, source_target_pairs={{0,4},{4,8},{8,12},{12,16},{16,20},{20,24},{24,28},{28,32},{32,36}... | collective-permute-start | bytes 49160 | tf_op jit(solution)/shard_map/ppermute | solution.py:37
  18.8 1.9 collective-permute-start.5
  20.8 0.7 fusion.32
  21.5 3.6 %collective-permute-start = (bf16[128,64]{0,1:T(8,128)(2,1)S(1)}, bf16[128,64]{0,1:T(8,128)(2,1)S(1)}, u32[]{:S(2)}, u32[]{:S(2)}) collective-permute-start(bf16[128,64]{0,1:T(8,128)(2,1)S(1)} %get-tuple-element.5), channel_id=1, source_target_pairs={{0,4},{4,8},{8,12},{12,16},{16,20},{20,24},{24,28},{28,32},{32,36}... | collective-permute-start | bytes 49160 | tf_op jit(solution)/shard_map/ppermute | solution.py:37
  25.3 1.3 reshape.98
  26.6 1.9 collective-permute-start.1
  29.0 0.9 pad_maximum_fusion.1
  30.0 0.4 slice.68
  31.6 0.4 collective-permute-done.1
  32.1 0.9 pad_maximum_fusion
  34.8 0.9 fusion.1
  35.8 0.9 fusion
  36.8 1.3 fusion.8
  38.6 13.1 %all_to_all.19 = bf16[4,128,256]{1,2,0:T(8,128)(2,1)S(1)} all-to-all(bf16[4,128,256]{1,2,0:T(8,128)(2,1)S(1)} %copy.44), channel_id=1, replica_groups=mesh['sp'=64,'tp'=4] {'tp'}, dimensions={0} | all-to-all | bytes 524288 | tf_op jit(solution)/shard_map/all_to_all | solution.py:402
  51.7 14.6 %all-gather.2.cloned.1.call-done = bf16[1024,2048]{1,0:T(8,128)(2,1)} async-done(((bf16[256,2048]{1,0:T(8,128)(2,1)}), bf16[1024,2048]{1,0:T(8,128)(2,1)}) %all-gather.2.cloned.1.call-update) | async-done | bytes 4194320 | tf_op jit(solution)/shard_map/all_gather | solution.py:405
  66.3 3.0 %fusion.11 = (f32[128]{0:T(128)S(1)}, bf16[128,2048]{1,0:T(8,128)(2,1)S(1)}) fusion(bf16[128,1024]{0,1:T(8,128)(2,1)S(1)} %bitcast.55, bf16[1024,2048]{1,0:T(8,128)(2,1)} %all-gather.2.cloned.1.call-done, bf16[128,2048]{1,0:T(8,128)(2,1)S(1)} %copy-done.1), kind=kOutput, calls=%fused_computation.13 | convolution fusion | flops 538443648 | bytes 5505536 | tf_op jit(solution)/shard_map/dot_general | solution.py:403
  69.4 1.0 fusion.13.normed
  70.4 158.9 %moe.1 = bf16[128,2048]{1,0:T(8,128)(2,1)} custom-call(bf16[128,2048]{1,0:T(8,128)(2,1)} %fusion.13.normed, bf16[128,2048]{1,0:T(8,128)(2,1)} %copy-done, s32[8,128]{1,0:T(8,128)} %bitcast.56, f32[8,128]{1,0:T(8,128)} %bitcast.57, bf16[1,2048,512]{2,1,0:T(8,128)(2,1)} %eg.1, bf16[1,2048,512]{2,1,0:T(8,128)(2,1)} %eu.1, bf16[1,512,2048]{2,1,0:T(8,128)(2,1)} %ed.1, ...), custom_call_target="tpu_custom_call" | custom-call | tf_op jit(solution)/shard_map/moe/pallas_call | solution.py:344
  229.3 1.9 copy.63
  (47 shorter events, 4.3 us)
Async XLA Ops:
  6.5 59.8 %all-gather.2.cloned.1.call-start = ((), (), s32[]{:S(2)}) async-start(), calls=%async_computation.1 | async-start | bytes 5242880 | tf_op jit(solution)/shard_map/all_gather | solution.py:405
  8.0 18.6 %collective-permute-start.2 = (bf16[128]{0:T(256)(128)(2,1)S(1)}, bf16[128]{0:T(256)(128)(2,1)S(1)}, u32[]{:S(2)}, u32[]{:S(2)}) collective-permute-start(bf16[128]{0:T(256)(128)(2,1)S(1)} %get-tuple-element.9), channel_id=1, source_target_pairs={{0,4},{4,8},{8,12},{12,16},{16,20},{20,24},{24,28},{28,32},{32,36}... | collective-permute-start | bytes 776 | tf_op jit(solution)/shard_map/ppermute | solution.py:37
  12.5 16.0 %collective-permute-start.3 = (bf16[128]{0:T(256)(128)(2,1)S(1)}, bf16[128]{0:T(256)(128)(2,1)S(1)}, u32[]{:S(2)}, u32[]{:S(2)}) collective-permute-start(bf16[128]{0:T(256)(128)(2,1)S(1)} %get-tuple-element.10), channel_id=1, source_target_pairs={{4,0},{8,4},{12,8},{16,12},{20,16},{24,20},{28,24},{32,28},{36,32}... | collective-permute-start | bytes 776 | tf_op jit(solution)/shard_map/ppermute | solution.py:39
  15.2 13.7 %collective-permute-start.4 = (bf16[128,64]{0,1:T(8,128)(2,1)S(1)}, bf16[128,64]{0,1:T(8,128)(2,1)S(1)}, u32[]{:S(2)}, u32[]{:S(2)}) collective-permute-start(bf16[128,64]{0,1:T(8,128)(2,1)S(1)} %get-tuple-element.7), channel_id=1, source_target_pairs={{0,4},{4,8},{8,12},{12,16},{16,20},{20,24},{24,28},{28,32},{32,36}... | collective-permute-start | bytes 49160 | tf_op jit(solution)/shard_map/ppermute | solution.py:37
  18.8 10.1 %collective-permute-start.5 = (bf16[128,64]{0,1:T(8,128)(2,1)S(1)}, bf16[128,64]{0,1:T(8,128)(2,1)S(1)}, u32[]{:S(2)}, u32[]{:S(2)}) collective-permute-start(bf16[128,64]{0,1:T(8,128)(2,1)S(1)} %get-tuple-element.8), channel_id=1, source_target_pairs={{4,0},{8,4},{12,8},{16,12},{20,16},{24,20},{28,24},{32,28},{36,32}... | collective-permute-start | bytes 49160 | tf_op jit(solution)/shard_map/ppermute | solution.py:39
  21.5 10.1 %collective-permute-start = (bf16[128,64]{0,1:T(8,128)(2,1)S(1)}, bf16[128,64]{0,1:T(8,128)(2,1)S(1)}, u32[]{:S(2)}, u32[]{:S(2)}) collective-permute-start(bf16[128,64]{0,1:T(8,128)(2,1)S(1)} %get-tuple-element.5), channel_id=1, source_target_pairs={{0,4},{4,8},{8,12},{12,16},{16,20},{20,24},{24,28},{28,32},{32,36}... | collective-permute-start | bytes 49160 | tf_op jit(solution)/shard_map/ppermute | solution.py:37
  25.3 10.4 %copy-start.3 = (f32[4]{0:T(128)S(1)}, f32[4]{0:T(128)}, u32[]{:S(2)}) copy-start(f32[4]{0:T(128)} %param.20) | copy-start | bytes 52
  26.6 5.5 %collective-permute-start.1 = (bf16[128,64]{0,1:T(8,128)(2,1)S(1)}, bf16[128,64]{0,1:T(8,128)(2,1)S(1)}, u32[]{:S(2)}, u32[]{:S(2)}) collective-permute-start(bf16[128,64]{0,1:T(8,128)(2,1)S(1)} %get-tuple-element.6), channel_id=1, source_target_pairs={{4,0},{8,4},{12,8},{16,12},{20,16},{24,20},{28,24},{32,28},{36,32}... | collective-permute-start | bytes 49160 | tf_op jit(solution)/shard_map/ppermute | solution.py:39
  36.8 29.5 %copy-start.1 = (bf16[128,2048]{1,0:T(8,128)(2,1)S(1)}, bf16[128,2048]{1,0:T(8,128)(2,1)}, u32[]{:S(2)}) copy-start(bf16[128,2048]{1,0:T(8,128)(2,1)} %param.22) | copy-start | bytes 1572868
  38.1 31.3 %copy-start.2 = (f32[2048]{0:T(1024)S(1)}, f32[2048]{0:T(1024)}, u32[]{:S(2)}) copy-start(f32[2048]{0:T(1024)} %param.23) | copy-start | bytes 24580
  69.4 1.0 copy-start
Sparse Core Ops, SparseCore 0:
  9.1 57.1 all-gather.1

commit v2 on v1

v2 whole, which is shorter than its diff:
```python
import functools

import jax
import jax.numpy as jnp
from jax import lax
from jax.experimental import pallas as pl
from jax.experimental.pallas import tpu as pltpu
from jax.sharding import PartitionSpec as P

HD = 64
WINDOW = 128
NZ, NY, NC, NX = 8, 4, 2, 4
PLANE = NY * NC
SP = NZ * PLANE
SPAN = 512
BLOCKS = SPAN // WINDOW
HEADS = 4
OUT_ROWS = HEADS * HD
ROWS = 128
HALF = 64
CAP = 12
SLOTS = 2 * CAP
PACK = PLANE * SLOTS
D = 2048
FF = 512
EXPERTS = 64
MESH = pl.DeviceIdType.MESH
BF = jnp.bfloat16
F32 = jnp.float32

norm_eps = 1e-06


def dot(a, b):
    return jnp.dot(a, b, preferred_element_type=F32)


def silu(v):
    return v / (1.0 + jnp.exp(-v))


def chunk_of(delta):
    return 0 if delta == 0 else (2 * delta - 1 if delta <= NZ // 2 else 2 * (NZ - delta))


def layer_kernel(
    q, k, v, docs, sink, wout, residual, gain, ids, weight, eg, eu, ed, shg, shu, shd, out,
    qv, ekv, edoc, attn, atf, wo, resid,
    tok, tx, rx, ret, rst, rsx, info, inf, wg, wu, wd, sg, su, sd, sacc, hid,
    h_s, h_r, a_s, a_r, o_s, o_r, f_s, f_r,
    z_s, z_r, i_s, i_r, d_s, d_r, e_s, e_r, p_s, p_r, x_s, x_r, w_s,
):
    sp, x = lax.axis_index("sp"), lax.axis_index("tp")
    z, mine = sp // PLANE, sp % PLANE
    core = sp % NC
    twin = (sp + 1 - 2 * core, x)

    def at_sp(step):
        return ((sp + step) % SP, x)

    def at_z(dz):
        return ((z + dz) % NZ * PLANE + mine, x)

    def at_plane(j):
        return (z * PLANE + j, x)

    def at_x(dx):
        return (sp, (x + dx) % NX)

    def send(src, dst, ssem, rsem, device):
        copy = pltpu.make_async_remote_copy(
            src_ref=src, dst_ref=dst, send_sem=ssem, recv_sem=rsem, device_id=device, device_id_type=MESH
        )
        copy.start()

    def landed(ref, sem):
        pltpu.make_async_copy(ref, ref, sem).wait()

    local = [
        pltpu.make_async_copy(q, qv, w_s.at[0]),
        pltpu.make_async_copy(wout, wo.at[0], w_s.at[1]),
        pltpu.make_async_copy(residual, resid, w_s.at[2]),
        pltpu.make_async_copy(shg, sg.at[0], w_s.at[3]),
        pltpu.make_async_copy(shu, su.at[0], w_s.at[4]),
        pltpu.make_async_copy(shd, sd.at[0], w_s.at[5]),
        pltpu.make_async_copy(eg.at[0], wg, w_s.at[6]),
        pltpu.make_async_copy(eu.at[0], wu, w_s.at[7]),
        pltpu.make_async_copy(ed.at[0], wd, w_s.at[8]),
    ]
    for copy in local:
        copy.start()

    barrier = pltpu.get_barrier_semaphore()
    peers = [at_z(dz) for dz in range(1, NZ)] + [at_x(dx) for dx in range(1, NX)]
    peers += [at_plane((mine + off) % PLANE) for off in range(1, PLANE)]
    peers += [at_sp(1), at_sp(SP - 1)]
    for device in peers:
        pl.semaphore_signal(barrier, inc=1, device_id=device, device_id_type=MESH)

    ekv[pl.ds(WINDOW, SPAN), :] = jnp.concatenate([k[...], v[...]], axis=1)
    for b in range(BLOCKS):
        edoc[b + 1] = jnp.broadcast_to(docs[b : b + 1, :].astype(F32), (8, ROWS))

    pl.semaphore_wait(barrier, len(peers))
    send(ekv.at[pl.ds(WINDOW, WINDOW)], ekv.at[pl.ds(WINDOW + SPAN, WINDOW)], h_s.at[0], h_r.at[0], at_sp(SP - 1))
    send(edoc.at[1], edoc.at[BLOCKS + 1], h_s.at[1], h_r.at[1], at_sp(SP - 1))
    send(ekv.at[pl.ds(SPAN, WINDOW)], ekv.at[pl.ds(0, WINDOW)], h_s.at[2], h_r.at[2], at_sp(1))
    send(edoc.at[BLOCKS], edoc.at[0], h_s.at[3], h_r.at[3], at_sp(1))
    own_half = pl.ds(pl.multiple_of(core * (OUT_ROWS // NC), OUT_ROWS // NC), OUT_ROWS // NC)
    local[1].wait()
    for dx in (1, 3, 2):
        send(wo.at[0, own_half], wo.at[dx, own_half], o_s.at[dx], o_r.at[dx], at_x(dx))

    expert = lax.broadcasted_iota(jnp.int32, (EXPERTS, ROWS), 0)
    hits = jnp.zeros((EXPERTS, ROWS), F32)
    wide = jnp.zeros((EXPERTS, ROWS), F32)
    for k in range(ids.shape[0]):
        named = ids[k : k + 1, :] == expert
        hits = hits + named.astype(F32)
        wide = wide + jnp.where(named, weight[k : k + 1, :], 0.0)
    row = lax.broadcasted_iota(jnp.int32, (ROWS, ROWS), 0)
    col = lax.broadcasted_iota(jnp.int32, (ROWS, ROWS), 1)
    earlier = ((row < col) & (row // HALF == col // HALF)).astype(BF)
    rank = dot(hits.astype(BF), earlier)
    half = lax.broadcasted_iota(jnp.int32, (EXPERTS, ROWS), 1) // HALF
    place = jnp.where(hits > 0.0, rank + (half * CAP).astype(F32), -1.0)
    for plane in range(NZ):
        lower = plane * PLANE
        info[plane, 0:PLANE, :] = place[lower : lower + PLANE]
        info[plane, PLANE : 2 * PLANE, :] = wide[lower : lower + PLANE]
    inf[0] = info[z]

    def attention(n, carry):
        b = jnp.where(n < 3, (n + 1) % 3, 3)

        @pl.when(n == 2)
        def _():
            landed(ekv.at[pl.ds(WINDOW + SPAN, WINDOW)], h_r.at[0])
            landed(edoc.at[BLOCKS + 1], h_r.at[1])
            landed(ekv.at[pl.ds(0, WINDOW)], h_r.at[2])
            landed(edoc.at[0], h_r.at[3])

            @pl.when(sp == 0)
            def _():
                edoc[0] = jnp.full((8, ROWS), -1.0, F32)

            @pl.when(sp == SP - 1)
            def _():
                edoc[BLOCKS + 1] = jnp.full((8, ROWS), -1.0, F32)

        rows = pl.ds(pl.multiple_of(b * WINDOW, WINDOW), WINDOW)
        band = ekv[pl.ds(pl.multiple_of(b * WINDOW, WINDOW), 3 * WINDOW), :]
        own_doc = jnp.broadcast_to(edoc[b + 1][0:1, :], (WINDOW, WINDOW)).T
        at_row = lax.broadcasted_iota(jnp.int32, (WINDOW, WINDOW), 0)
        at_col = lax.broadcasted_iota(jnp.int32, (WINDOW, WINDOW), 1)
        near = (at_col >= at_row, at_row >= 0, at_col <= at_row)
        allowed = jnp.concatenate(
            [
                ((own_doc == edoc[b + t][0:1, :]) & near[t]).astype(F32)
                for t in range(3)
            ],
            axis=1,
        )
        heads = []
        for h in range(HEADS):
            query = qv[rows, h * HD : (h + 1) * HD]
            scores = lax.dot_general(
                query, band[:, :HD], (((1,), (1,)), ((), ())), preferred_element_type=F32
            ) * HD ** (-0.5)
            scores = jnp.where(allowed > 0.0, scores, -jnp.inf)
            row_max = jnp.maximum(jnp.max(scores, axis=1, keepdims=True), sink[h])
            grown = jnp.exp(scores - row_max)
            total = jnp.sum(grown, axis=1, keepdims=True) + jnp.exp(sink[h] - row_max)
            heads.append(dot((grown / total).astype(BF), band[:, HD:]).astype(BF))
        attn[b] = jnp.concatenate(heads, axis=1)
        slot = (b + NX - x) % NX

        @pl.when(b != x)
        def _():
            send(attn.at[b], atf.at[slot], a_s.at[slot], a_r.at[slot], (sp, b))

        @pl.when(b == x)
        def _():
            pltpu.make_async_copy(attn.at[b], atf.at[0], a_r.at[0]).start()

        return carry

    local[0].wait()
    lax.fori_loop(0, BLOCKS, attention, 0)

    for dx in (1, 3, 2):
        landed(wo.at[dx, own_half], o_r.at[dx])
        send(wo.at[dx, own_half], wo.at[dx, own_half], f_s.at[dx], f_r.at[dx], twin)
    local[2].wait()
    other_half = pl.ds(
        pl.multiple_of((1 - core) * (OUT_ROWS // NC), OUT_ROWS // NC), OUT_ROWS // NC
    )
    landed(atf.at[0], a_r.at[0])
    for dx in (1, 3, 2):
        landed(atf.at[dx], a_r.at[dx])
        landed(wo.at[dx, other_half], f_r.at[dx])

    def project(n, squares):
        cols = pl.ds(pl.multiple_of(n * 256, 256), 256)
        mixed = dot(atf[0], wo[0, :, cols])
        for dx in range(1, NX):
            mixed = mixed + dot(atf[dx], wo[dx, :, cols])
        rounded = (resid[:, cols].astype(F32) + mixed).astype(BF)
        resid[:, cols] = rounded
        squared = rounded.astype(F32)
        squared = squared * squared
        return squares + squared[:, :128] + squared[:, 128:]

    squares = lax.fori_loop(0, D // 256, project, jnp.zeros((ROWS, 128), F32))
    scale = lax.rsqrt(jnp.sum(squares, axis=1, keepdims=True) * (1.0 / D) + norm_eps)
    for n in range(D // 512):
        cols = pl.ds(n * 512, 512)
        tok[0, :, cols] = (resid[:, cols].astype(F32) * scale * gain[:, cols]).astype(BF)

    for delta in range(1, NZ):
        i = chunk_of(delta)
        send(info.at[(z + delta) % NZ], inf.at[i], i_s.at[i], i_r.at[i], at_z(delta))
    send(tok.at[0], tok.at[1], z_s.at[1], z_r.at[1], at_z(1))
    send(tok.at[0], tok.at[2], z_s.at[2], z_r.at[2], at_z(NZ - 1))

    def placed(i):
        slot = lax.broadcasted_iota(jnp.int32, (PLANE, SLOTS, ROWS), 1).astype(F32)
        return (inf[i, 0:PLANE, :][:, None, :] == slot).astype(F32)

    def dispatch(i):
        @pl.when(i > 0)
        def _():
            landed(tok.at[i], z_r.at[i])
            landed(inf.at[i], i_r.at[i])

        @pl.when((i > 0) & (i + 2 < NZ))
        def _():
            way = 1 + (NZ - 2) * ((i + 1) % 2)
            send(tok.at[i], tok.at[i + 2], z_s.at[i + 2], z_r.at[i + 2], at_z(way))

        pick = placed(i).reshape(PACK, ROWS).astype(BF)
        for n in range(D // 512):
            cols = pl.ds(n * 512, 512)
            tx[i, :, :, cols] = dot(pick, tok[i, :, cols]).astype(BF).reshape(PLANE, SLOTS, 512)
        for off in range(1, PLANE):
            j = (mine + off) % PLANE
            send(tx.at[i, j], rx.at[i, mine], d_s.at[i], d_r.at[i], at_plane(j))
        pltpu.make_async_copy(tx.at[i, mine], rx.at[i, mine], d_r.at[i]).start()

    def run_expert(i):
        landed(rx.at[i], d_r.at[i])

        def hidden_tile(n, carry):
            cols = pl.ds(pl.multiple_of(n * 256, 256), 256)
            rows = rx[i].reshape(PACK, D)
            hid[:, cols] = (silu(dot(rows, wg[:, cols])) * dot(rows, wu[:, cols])).astype(BF)
            return carry

        lax.fori_loop(0, FF // 256, hidden_tile, 0)

        def out_tile(n, carry):
            cols = pl.ds(pl.multiple_of(n * 512, 512), 512)
            rx[i, :, :, cols] = dot(hid[...], wd[:, cols]).astype(BF).reshape(PLANE, SLOTS, 512)
            return carry

        lax.fori_loop(0, D // 512, out_tile, 0)

    def give_back(i):
        for off in range(1, PLANE):
            j = (mine + off) % PLANE
            send(rx.at[i, j], ret.at[i, mine], e_s.at[i], e_r.at[i], at_plane(j))
        pltpu.make_async_copy(rx.at[i, mine], ret.at[i, mine], e_r.at[i]).start()

    LAG = 2

    def forward(i, carry):
        @pl.when(i < NZ)
        def _():
            dispatch(i)

        @pl.when(i == 0)
        def _():
            for dx in range(1, NX):
                send(sg.at[0], sg.at[dx], x_s.at[0, dx], x_r.at[0, dx], at_x(dx))
                send(su.at[0], su.at[dx], x_s.at[1, dx], x_r.at[1, dx], at_x(dx))
                send(sd.at[0], sd.at[dx], x_s.at[2, dx], x_r.at[2, dx], at_x(dx))

        @pl.when(i >= LAG)
        def _():
            run_expert(i - LAG)

        @pl.when(i >= NZ - 2 + LAG)
        def _():
            give_back(i - LAG)

        return carry

    for copy in local[3:]:
        copy.wait()
    lax.fori_loop(0, NZ + LAG, forward, 0)

    def backward(n, carry):
        give_back(NZ - 3 - n)
        return carry

    lax.fori_loop(0, NZ - 2, backward, 0)

    for dx in range(1, NX):
        landed(sg.at[dx], x_r.at[0, dx])
        landed(su.at[dx], x_r.at[1, dx])
        landed(sd.at[dx], x_r.at[2, dx])
    sacc[...] = jnp.zeros_like(sacc)

    def shared_block(dx, carry):
        rows = tok[0]
        units = (silu(dot(rows, sg[dx])) * dot(rows, su[dx])).astype(BF)
        for n in range(D // 512):
            cols = pl.ds(n * 512, 512)
            sacc[:, cols] = sacc[:, cols] + dot(units, sd[dx, :, cols])
        return carry

    lax.fori_loop(0, NX, shared_block, 0)

    def combined(i):
        landed(ret.at[i], e_r.at[i])
        scaled = placed(i) * inf[i, PLANE : 2 * PLANE, :][:, None, :]
        scaled = jnp.concatenate([scaled.reshape(PACK, ROWS), jnp.zeros((256 - PACK, ROWS), F32)], axis=0)
        scaled = scaled.T[:, :PACK]
        high = scaled.astype(BF)
        low = (scaled - high.astype(F32)).astype(BF)

        def part(cols):
            rows = ret[i, :, :, cols].reshape(PACK, 512)
            return dot(high, rows) + dot(low, rows)

        return part

    def pass_on(i):
        way = NZ - 1 - (NZ - 2) * ((i + 1) % 2)
        send(rst.at[i], rsx.at[i], p_s.at[i], p_r.at[i], at_z(way))

    def farthest(n, carry):
        i = NZ - 1 - n
        part = combined(i)
        for n in range(D // 512):
            cols = pl.ds(n * 512, 512)
            rst[i, :, cols] = part(cols).astype(BF)
        pass_on(i)
        return carry

    lax.fori_loop(0, 2, farthest, 0)

    def nearer(n, carry):
        i = NZ - 3 - n
        part = combined(i)
        landed(rsx.at[i + 2], p_r.at[i + 2])
        for n in range(D // 512):
            cols = pl.ds(n * 512, 512)
            rst[i, :, cols] = (part(cols) + rsx[i + 2, :, cols].astype(F32)).astype(BF)
        pass_on(i)
        return carry

    lax.fori_loop(0, NZ - 3, nearer, 0)

    part = combined(0)
    landed(rsx.at[2], p_r.at[2])
    landed(rsx.at[1], p_r.at[1])
    for n in range(D // 512):
        cols = pl.ds(n * 512, 512)
        routed = part(cols) + rsx[2, :, cols].astype(F32) + rsx[1, :, cols].astype(F32)
        out[:, cols] = (resid[:, cols].astype(F32) + sacc[:, cols] + routed).astype(BF)

    for i in range(NZ):
        landed(tx.at[i, pl.ds(0, PLANE - 1)], d_s.at[i])
        landed(rx.at[i, pl.ds(0, PLANE - 1)], e_s.at[i])
        if i > 0:
            landed(tok.at[i], z_s.at[i])
            landed(info.at[i], i_s.at[i])
            landed(rst.at[i], p_s.at[i])
    landed(ekv.at[pl.ds(0, WINDOW)], h_s.at[0])
    landed(edoc.at[0], h_s.at[1])
    landed(ekv.at[pl.ds(0, WINDOW)], h_s.at[2])
    landed(edoc.at[0], h_s.at[3])
    for dx in range(1, NX):
        landed(atf.at[0], a_s.at[dx])
        landed(wo.at[0, pl.ds(0, OUT_ROWS // NC)], o_s.at[dx])
        landed(wo.at[0, pl.ds(0, OUT_ROWS // NC)], f_s.at[dx])
        landed(sg.at[0], x_s.at[0, dx])
        landed(su.at[0], x_s.at[1, dx])
        landed(sd.at[0], x_s.at[2, dx])


def shards(
    queries,
    keys,
    values,
    doc_ids,
    sink_logit,
    w_out,
    residual,
    ffn_gain,
    expert_ids,
    expert_weight,
    exp_gate,
    exp_up,
    exp_down,
    shared_gate,
    shared_up,
    shared_down,
):
    vmem = pl.BlockSpec(memory_space=pltpu.VMEM)
    smem = pl.BlockSpec(memory_space=pltpu.SMEM)
    hbm = pl.BlockSpec(memory_space=pl.ANY)
    dma = pltpu.SemaphoreType.DMA
    unit = FF // NX
    return pl.pallas_call(
        layer_kernel,
        out_shape=jax.ShapeDtypeStruct((ROWS, D), BF),
        in_specs=[hbm, vmem, vmem, vmem, smem, hbm, hbm, vmem, vmem, vmem] + [hbm] * 6,
        out_specs=vmem,
        scratch_shapes=[
            pltpu.VMEM((SPAN, HEADS * HD), BF),
            pltpu.VMEM((SPAN + 2 * WINDOW, 2 * HD), BF),
            pltpu.VMEM((BLOCKS + 2, 8, ROWS), F32),
            pltpu.VMEM((BLOCKS, ROWS, HEADS * HD), BF),
            pltpu.VMEM((NX, ROWS, HEADS * HD), BF),
            pltpu.VMEM((NX, OUT_ROWS, D), BF),
            pltpu.VMEM((ROWS, D), BF),
            pltpu.VMEM((NZ, ROWS, D), BF),
            pltpu.VMEM((NZ, PLANE, SLOTS, D), BF),
            pltpu.VMEM((NZ, PLANE, SLOTS, D), BF),
            pltpu.VMEM((NZ, PLANE, SLOTS, D), BF),
            pltpu.VMEM((NZ, ROWS, D), BF),
            pltpu.VMEM((NZ, ROWS, D), BF),
            pltpu.VMEM((NZ, 2 * PLANE, ROWS), F32),
            pltpu.VMEM((NZ, 2 * PLANE, ROWS), F32),
            pltpu.VMEM((D, FF), BF),
            pltpu.VMEM((D, FF), BF),
            pltpu.VMEM((FF, D), BF),
            pltpu.VMEM((NX, D, unit), BF),
            pltpu.VMEM((NX, D, unit), BF),
            pltpu.VMEM((NX, unit, D), BF),
            pltpu.VMEM((ROWS, D), F32),
            pltpu.VMEM((PACK, FF), BF),
        ]
        + [dma((4,))] * 8
        + [dma((NZ,))] * 10
        + [dma((3, NX)), dma((3, NX)), dma((9,))],
        compiler_params=pltpu.CompilerParams(
            collective_id=1, has_side_effects=True, vmem_limit_bytes=62 * 2**20
        ),
        name="layer",
    )(
        queries, keys, values, doc_ids.reshape(BLOCKS, ROWS), sink_logit, w_out, residual,
        ffn_gain.reshape(1, D), expert_ids.T, expert_weight.T,
        exp_gate, exp_up, exp_down, shared_gate, shared_up, shared_down,
    )


def solution(mesh):
    placed = (
        P("sp", "tp"),
        P("sp", "tp"),
        P("sp", "tp"),
        P("sp"),
        P("tp"),
        P("tp", None),
        P(("sp", "tp"), None),
        P(),
        P(("sp", "tp"), None),
        P(("sp", "tp"), None),
        P("sp", None, None),
        P("sp", None, None),
        P("sp", None, None),
        P(None, "tp"),
        P(None, "tp"),
        P("tp", None),
    )
    return jax.shard_map(
        shards, mesh=mesh, in_specs=placed, out_specs=P(("sp", "tp"), None), check_vma=False
    )
```

time: 239 us -> 198 us (0.83)
  Pallas kernels: 159 us -> 193 us
  starting transfers between devices: 17.6 us -> 0 us
  waiting for transfers between devices: 15.8 us -> 0 us
  between operations: 13.7 us -> 0.01 us
  blocking collectives: 13.1 us -> 0 us
  matrix products: 5.21 us -> 0 us
  other arithmetic: 4.85 us -> 0 us
  local copies, waits for them, and re-layouts: 8.82 us -> 5.07 us
    pallas_call x1, Pallas kernels: 159 us -> 193 us  [shards(): pl.pallas_call(layer_kernel, out_shape=jax.ShapeDtypeStruct((ROWS, D), BF...]
    ppermute x6 -> x0, starting transfers between devices: 17.6 us -> none  [the longest x3 11.8 us: extended(): lax.ppermute(tail, axis, [(i, (i + 1) % count) for i in range(ends)])]
    all_gather x1 -> x0, waiting for transfers between devices: 14.6 us -> none  [shards(): lax.all_gather(w_out, 'tp', axis=0, tiled=True)]
    all_to_all x1 -> x0, blocking collectives: 13.1 us -> none  [shards(): lax.all_to_all(attended, 'tp', split_axis=0, concat_axis=1, tiled=True)]
    dot_general x3 -> x0, matrix products: 5.21 us -> none  [the longest x1 3.03 us: shards(): jnp.dot(own_rows, lax.all_gather(w_out, 'tp', axis=0, tiled=True), prefer...]
    slice x15 -> x0, local copies, waits for them, and re-layouts: 4.82 us -> none  [the longest x3 1.49 us: extended(): lax.slice_in_dim(cells, cells.shape[dim] - width, cells.shape[dim], axis=...]
    unnamed x17 -> x3, local copies, waits for them, and re-layouts: 1.96 us -> 5.07 us
  transfers between devices with their start and end apart: 7 -> 0, of which waited for: 2 -> 0; matrix products, arithmetic and copies ran while one was open for 5% -> 0% of each run, Pallas kernels for 0% -> 0%
where the time goes in v2:
time: 198 us
  Pallas kernels  193 us (97%)
  local copies, waits for them, and re-layouts  5.07 us (3%)
    pallas_call x1, Pallas kernels, shards(): pl.pallas_call(layer_kernel, out_shape=jax.ShapeDtypeStruct((ROWS, D), BF...  193 us
    unnamed x3, local copies, waits for them, and re-layouts  5.07 us

profile of v2, /device:TPU:1, one launch (start us, length us, event | category | flops | bytes accessed | tf_op | source)
XLA Modules:
  0.0 198.1 jit_solution(8844102225501864466)
XLA Ops:
  0.0 1.6 copy.17.k
  1.6 1.6 copy.18.v
  3.2 193.0 %layer.1 = bf16[128,2048]{1,0:T(8,128)(2,1)} custom-call(bf16[512,256]{1,0:T(8,128)(2,1)} %q.1, bf16[512,64]{1,0:T(8,128)(2,1)} %copy.17.k, bf16[512,64]{1,0:T(8,128)(2,1)} %copy.18.v, s32[4,128]{1,0:T(4,128)} %bitcast.7, f32[4]{0:T(128)} %sink.1, bf16[256,2048]{1,0:T(8,128)(2,1)} %wout.1, bf16[128,2048]{1,0:T(8,128)(2,1)} %residual.1, f32[1,2048]{1,0:T(1,128)} %bitcast.4, ...), custom_call_target="tpu_custom_call" | custom-call | tf_op jit(solution)/shard_map/layer/pallas_call | solution.py:416
  196.2 1.9 copy.20

commit v3 on v2

v3 whole, which is shorter than its diff:
```python
import functools

import jax
import jax.numpy as jnp
from jax import lax
from jax.experimental import pallas as pl
from jax.experimental.pallas import tpu as pltpu
from jax.sharding import PartitionSpec as P

HD = 64
WINDOW = 128
NZ, NY, NC, NX = 8, 4, 2, 4
PLANE = NY * NC
SP = NZ * PLANE
SPAN = 512
BLOCKS = SPAN // WINDOW
HEADS = 4
OUT_ROWS = HEADS * HD
OUT_HALF = OUT_ROWS // NC
DIRECT = 64
SHARE = (OUT_HALF - DIRECT) // NY
PART = 1024
ROWS = 128
HALF = 64
CAP = 12
SLOTS = 2 * CAP
PACK = PLANE * SLOTS
D = 2048
FF = 512
EXPERTS = 64
MESH = pl.DeviceIdType.MESH
BF = jnp.bfloat16
F32 = jnp.float32

norm_eps = 1e-06


def dot(a, b):
    return jnp.dot(a, b, preferred_element_type=F32)


def silu(v):
    return v / (1.0 + jnp.exp(-v))


def chunk_of(delta):
    return 0 if delta == 0 else (2 * delta - 1 if delta <= NZ // 2 else 2 * (NZ - delta))


def layer_kernel(
    q, k, v, docs, sink, wout, residual, gain, ids, weight, eg, eu, ed, shg, shu, shd, out,
    qv, ekv, edoc, attn, atf, wo, resid,
    tok, tx, rx, ret, rst, rsx, info, inf, wg, wu, wd, sg, su, sd, sacc, hid,
    h_s, h_r, a_s, a_r, o_s, o_r, f_s, f_r, g_s, g_r,
    z_s, z_r, i_s, i_r, d_s, d_r, e_s, e_r, p_s, p_r, x_s, x_r, w_s,
):
    sp, x = lax.axis_index("sp"), lax.axis_index("tp")
    z, mine = sp // PLANE, sp % PLANE
    core = sp % NC
    twin = (sp + 1 - 2 * core, x)

    def at_sp(step):
        return ((sp + step) % SP, x)

    def at_z(dz):
        return ((z + dz) % NZ * PLANE + mine, x)

    def at_plane(j):
        return (z * PLANE + j, x)

    def at_x(dx):
        return (sp, (x + dx) % NX)

    def send(src, dst, ssem, rsem, device):
        copy = pltpu.make_async_remote_copy(
            src_ref=src, dst_ref=dst, send_sem=ssem, recv_sem=rsem, device_id=device, device_id_type=MESH
        )
        copy.start()

    def landed(ref, sem):
        pltpu.make_async_copy(ref, ref, sem).wait()

    local = [
        pltpu.make_async_copy(q, qv, w_s.at[0]),
        pltpu.make_async_copy(residual, resid, w_s.at[1]),
        pltpu.make_async_copy(wout, wo.at[0], w_s.at[2]),
        pltpu.make_async_copy(shg, sg.at[0], w_s.at[3]),
        pltpu.make_async_copy(shu, su.at[0], w_s.at[4]),
        pltpu.make_async_copy(shd, sd.at[0], w_s.at[5]),
        pltpu.make_async_copy(eg.at[0], wg, w_s.at[6]),
        pltpu.make_async_copy(eu.at[0], wu, w_s.at[7]),
        pltpu.make_async_copy(ed.at[0], wd, w_s.at[8]),
    ]
    for copy in local[:2]:
        copy.start()

    barrier = pltpu.get_barrier_semaphore()
    peers = [at_z(dz) for dz in range(1, NZ)] + [at_x(dx) for dx in range(1, NX)]
    peers += [at_plane((mine + off) % PLANE) for off in range(1, PLANE)]
    peers += [at_sp(1), at_sp(SP - 1)]
    for device in peers:
        pl.semaphore_signal(barrier, inc=1, device_id=device, device_id_type=MESH)

    ekv[0:HD, pl.ds(WINDOW, SPAN)] = k[...]
    ekv[HD : 2 * HD, pl.ds(WINDOW, SPAN)] = v[...]
    for b in range(BLOCKS):
        edoc[b + 1] = jnp.broadcast_to(docs[b : b + 1, :].astype(F32), (8, ROWS))

    pl.semaphore_wait(barrier, len(peers))
    send(ekv.at[:, pl.ds(WINDOW, WINDOW)], ekv.at[:, pl.ds(WINDOW + SPAN, WINDOW)], h_s.at[0], h_r.at[0], at_sp(SP - 1))
    send(edoc.at[1], edoc.at[BLOCKS + 1], h_s.at[1], h_r.at[1], at_sp(SP - 1))
    send(ekv.at[:, pl.ds(SPAN, WINDOW)], ekv.at[:, pl.ds(0, WINDOW)], h_s.at[2], h_r.at[2], at_sp(1))
    send(edoc.at[BLOCKS], edoc.at[0], h_s.at[3], h_r.at[3], at_sp(1))
    lower = core * OUT_HALF
    direct = pl.ds(pl.multiple_of(lower, OUT_HALF), DIRECT)
    spread = pl.ds(pl.multiple_of(lower + DIRECT, SHARE), OUT_HALF - DIRECT)
    share = pl.ds(pl.multiple_of(lower + DIRECT + mine // NC * SHARE, SHARE), SHARE)
    others = pl.ds(1, NX - 1)
    for dx in (1, 3, 2):
        send(wout.at[share], wo.at[dx, share], g_s.at[0, dx], g_r.at[0, dx], at_x(dx))
    for dx in (1, 3, 2):
        send(wout.at[direct], wo.at[dx, direct], o_s.at[dx], o_r.at[dx], at_x(dx))

    expert = lax.broadcasted_iota(jnp.int32, (EXPERTS, ROWS), 0)
    hits = jnp.zeros((EXPERTS, ROWS), F32)
    wide = jnp.zeros((EXPERTS, ROWS), F32)
    for k in range(ids.shape[0]):
        named = ids[k : k + 1, :] == expert
        hits = hits + named.astype(F32)
        wide = wide + jnp.where(named, weight[k : k + 1, :], 0.0)
    row = lax.broadcasted_iota(jnp.int32, (ROWS, ROWS), 0)
    col = lax.broadcasted_iota(jnp.int32, (ROWS, ROWS), 1)
    earlier = ((row < col) & (row // HALF == col // HALF)).astype(BF)
    rank = dot(hits.astype(BF), earlier)
    half = lax.broadcasted_iota(jnp.int32, (EXPERTS, ROWS), 1) // HALF
    place = jnp.where(hits > 0.0, rank + (half * CAP).astype(F32), -1.0)
    for plane in range(NZ):
        lower = plane * PLANE
        info[plane, 0:PLANE, :] = place[lower : lower + PLANE]
        info[plane, PLANE : 2 * PLANE, :] = wide[lower : lower + PLANE]
    inf[0] = info[z]

    def attention(n, carry):
        b = jnp.where(n < 3, (n + 1) % 3, 3)

        @pl.when(n == 2)
        def _():
            landed(ekv.at[:, pl.ds(WINDOW + SPAN, WINDOW)], h_r.at[0])
            landed(edoc.at[BLOCKS + 1], h_r.at[1])
            landed(ekv.at[:, pl.ds(0, WINDOW)], h_r.at[2])
            landed(edoc.at[0], h_r.at[3])

            @pl.when(sp == 0)
            def _():
                edoc[0] = jnp.full((8, ROWS), -1.0, F32)

            @pl.when(sp == SP - 1)
            def _():
                edoc[BLOCKS + 1] = jnp.full((8, ROWS), -1.0, F32)

        rows = pl.ds(pl.multiple_of(b * WINDOW, WINDOW), WINDOW)
        band = ekv[:, pl.ds(pl.multiple_of(b * WINDOW, WINDOW), 3 * WINDOW)]
        own_doc = jnp.broadcast_to(edoc[b + 1][0:1, :], (WINDOW, WINDOW)).T
        at_row = lax.broadcasted_iota(jnp.int32, (WINDOW, WINDOW), 0)
        at_col = lax.broadcasted_iota(jnp.int32, (WINDOW, WINDOW), 1)
        near = (at_col >= at_row, at_row >= 0, at_col <= at_row)
        allowed = jnp.concatenate(
            [
                ((own_doc == edoc[b + t][0:1, :]) & near[t]).astype(F32)
                for t in range(3)
            ],
            axis=1,
        )
        heads = []
        for h in range(HEADS):
            query = qv[rows, h * HD : (h + 1) * HD]
            scores = dot(query, band[:HD]) * HD ** (-0.5)
            scores = jnp.where(allowed > 0.0, scores, -jnp.inf)
            row_max = jnp.maximum(jnp.max(scores, axis=1, keepdims=True), sink[h])
            grown = jnp.exp(scores - row_max)
            total = jnp.sum(grown, axis=1, keepdims=True) + jnp.exp(sink[h] - row_max)
            probs = (grown / total).astype(BF)
            mixed = lax.dot_general(probs, band[HD:], (((1,), (1,)), ((), ())), preferred_element_type=F32)
            heads.append(mixed.astype(BF))
        attn[b] = jnp.concatenate(heads, axis=1)
        slot = (b + NX - x) % NX

        @pl.when(b != x)
        def _():
            send(attn.at[b], atf.at[slot], a_s.at[slot], a_r.at[slot], (sp, b))

        @pl.when(b == x)
        def _():
            pltpu.make_async_copy(attn.at[b], atf.at[0], a_r.at[0]).start()

        return carry

    local[0].wait()
    lax.fori_loop(0, BLOCKS, attention, 0)

    for copy in local[2:]:
        copy.start()
    for dx in (1, 3, 2):
        landed(wo.at[dx, share], g_r.at[0, dx])
    for dy in range(1, NY):
        send(wo.at[others, share], wo.at[others, share], g_s.at[1, dy], g_r.at[1, dy], at_plane((mine + NC * dy) % PLANE))
    for dx in (1, 3, 2):
        landed(wo.at[dx, direct], o_r.at[dx])
    send(wo.at[others, direct], wo.at[others, direct], f_s.at[0], f_r.at[0], twin)
    for dy in range(1, NY):
        landed(wo.at[others, share], g_r.at[1, dy])
    send(wo.at[others, spread], wo.at[others, spread], f_s.at[1], f_r.at[1], twin)
    local[1].wait()
    local[2].wait()
    for dx in range(NX):
        landed(atf.at[dx], a_r.at[dx])
    landed(wo.at[others, direct], f_r.at[0])
    landed(wo.at[others, spread], f_r.at[1])

    def project(n, squares):
        cols = pl.ds(pl.multiple_of(n * 256, 256), 256)
        mixed = dot(atf[0], wo[0, :, cols])
        for dx in range(1, NX):
            mixed = mixed + dot(atf[dx], wo[dx, :, cols])
        rounded = (resid[:, cols].astype(F32) + mixed).astype(BF)
        resid[:, cols] = rounded
        squared = rounded.astype(F32)
        squared = squared * squared
        return squares + squared[:, :128] + squared[:, 128:]

    squares = lax.fori_loop(0, D // 256, project, jnp.zeros((ROWS, 128), F32))
    scale = lax.rsqrt(jnp.sum(squares, axis=1, keepdims=True) * (1.0 / D) + norm_eps)
    for h in range(2):
        cols = pl.ds(h * PART, PART)
        tok[0, h] = (resid[:, cols].astype(F32) * scale * gain[:, cols]).astype(BF)

    for delta in range(1, NZ):
        i = chunk_of(delta)
        send(info.at[(z + delta) % NZ], inf.at[i], i_s.at[i], i_r.at[i], at_z(delta))
    for h in range(2):
        send(tok.at[0, h], tok.at[1, h], z_s.at[1, h], z_r.at[1, h], at_z(1))
        send(tok.at[0, h], tok.at[2, h], z_s.at[2, h], z_r.at[2, h], at_z(NZ - 1))

    def placed(i):
        slot = lax.broadcasted_iota(jnp.int32, (PLANE, SLOTS, ROWS), 1).astype(F32)
        return (inf[i, 0:PLANE, :][:, None, :] == slot).astype(F32)

    def dispatch(i, h):
        @pl.when(i > 0)
        def _():
            landed(tok.at[i, h], z_r.at[i, h])

            @pl.when(h == 0)
            def _():
                landed(inf.at[i], i_r.at[i])

        @pl.when((i > 0) & (i + 2 < NZ))
        def _():
            way = 1 + (NZ - 2) * ((i + 1) % 2)
            send(tok.at[i, h], tok.at[i + 2, h], z_s.at[i + 2, h], z_r.at[i + 2, h], at_z(way))

        pick = placed(i).reshape(PACK, ROWS).astype(BF)
        for n in range(PART // 512):
            cols = pl.ds(n * 512, 512)
            tx[i, h, :, :, cols] = dot(pick, tok[i, h, :, cols]).astype(BF).reshape(PLANE, SLOTS, 512)
        for off in range(1, PLANE):
            j = (mine + off) % PLANE
            send(tx.at[i, h, j], rx.at[i, h, mine], d_s.at[i], d_r.at[i], at_plane(j))
        pltpu.make_async_copy(tx.at[i, h, mine], rx.at[i, h, mine], d_r.at[i]).start()

    def run_expert(i):
        landed(rx.at[i], d_r.at[i])

        def hidden_tile(n, carry):
            cols = pl.ds(pl.multiple_of(n * 256, 256), 256)
            left, right = rx[i, 0].reshape(PACK, PART), rx[i, 1].reshape(PACK, PART)
            gate = dot(left, wg[0:PART, cols]) + dot(right, wg[PART:D, cols])
            up = dot(left, wu[0:PART, cols]) + dot(right, wu[PART:D, cols])
            hid[:, cols] = (silu(gate) * up).astype(BF)
            return carry

        lax.fori_loop(0, FF // 256, hidden_tile, 0)

        def out_tile(n, carry):
            cols = pl.ds(pl.multiple_of(n * 512, 512), 512)
            made = dot(hid[...], wd[:, cols]).astype(BF).reshape(PLANE, SLOTS, 512)
            rx[i, n // 2, :, :, pl.ds(pl.multiple_of(n % 2 * 512, 512), 512)] = made
            return carry

        lax.fori_loop(0, D // 512, out_tile, 0)

    def give_back(i):
        for h in range(2):
            for off in range(1, PLANE):
                j = (mine + off) % PLANE
                send(rx.at[i, h, j], ret.at[i, h, mine], e_s.at[i, h], e_r.at[i, h], at_plane(j))
            pltpu.make_async_copy(rx.at[i, h, mine], ret.at[i, h, mine], e_r.at[i, h]).start()

    def pieces(n, carry):
        m = jnp.maximum(n - 2, 0)
        i = jnp.where(n < 2, 0, 1 + m // 4 * 2 + m % 2)
        h = jnp.where(n < 2, n, m % 4 // 2)

        @pl.when(i < NZ)
        def _():
            dispatch(i, h)

        @pl.when(n == 1)
        def _():
            for copy in local[3:6]:
                copy.wait()
            for dx in range(1, NX):
                send(sg.at[0], sg.at[dx], x_s.at[0, dx], x_r.at[0, dx], at_x(dx))
                send(su.at[0], su.at[dx], x_s.at[1, dx], x_r.at[1, dx], at_x(dx))
                send(sd.at[0], sd.at[dx], x_s.at[2, dx], x_r.at[2, dx], at_x(dx))
            for copy in local[6:]:
                copy.wait()

        @pl.when((n == 9) | (n == 13))
        def _():
            def early(j, carry):
                run_expert((n - 9) // 2 + j)
                return carry

            lax.fori_loop(0, 2, early, 0)

        return carry

    lax.fori_loop(0, 2 + 2 * NZ, pieces, 0)

    def late(j, carry):
        run_expert(j)

        @pl.when(j >= NZ - 2)
        def _():
            give_back(j)

        return carry

    lax.fori_loop(4, NZ, late, 0)

    def backward(n, carry):
        give_back(NZ - 3 - n)
        return carry

    lax.fori_loop(0, NZ - 2, backward, 0)

    for dx in range(1, NX):
        landed(sg.at[dx], x_r.at[0, dx])
        landed(su.at[dx], x_r.at[1, dx])
        landed(sd.at[dx], x_r.at[2, dx])
    sacc[...] = jnp.zeros_like(sacc)

    def shared_block(dx, carry):
        left, right = tok[0, 0], tok[0, 1]
        gate = dot(left, sg[dx, 0:PART]) + dot(right, sg[dx, PART:D])
        up = dot(left, su[dx, 0:PART]) + dot(right, su[dx, PART:D])
        units = (silu(gate) * up).astype(BF)
        for n in range(D // 512):
            cols = pl.ds(n * 512, 512)
            sacc[:, cols] = sacc[:, cols] + dot(units, sd[dx, :, cols])
        return carry

    lax.fori_loop(0, NX, shared_block, 0)

    def combined(i):
        scaled = placed(i) * inf[i, PLANE : 2 * PLANE, :][:, None, :]
        scaled = jnp.concatenate([scaled.reshape(PACK, ROWS), jnp.zeros((256 - PACK, ROWS), F32)], axis=0)
        scaled = scaled.T[:, :PACK]
        high = scaled.astype(BF)
        low = (scaled - high.astype(F32)).astype(BF)

        def part(h, cols):
            rows = ret[i, h, :, :, cols].reshape(PACK, 512)
            return dot(high, rows) + dot(low, rows)

        return part

    def pass_on(i, h):
        way = NZ - 1 - (NZ - 2) * ((i + 1) % 2)
        send(rst.at[i, h], rsx.at[i, h], p_s.at[i, h], p_r.at[i, h], at_z(way))

    def farthest(n, carry):
        i = NZ - 2 + n
        part = combined(i)
        for h in range(2):
            landed(ret.at[i, h], e_r.at[i, h])
            for n in range(PART // 512):
                cols = pl.ds(n * 512, 512)
                rst[i, h, :, cols] = part(h, cols).astype(BF)
            pass_on(i, h)
        return carry

    lax.fori_loop(0, 2, farthest, 0)

    def nearer(n, carry):
        i = NZ - 3 - n
        part = combined(i)
        for h in range(2):
            landed(ret.at[i, h], e_r.at[i, h])
            landed(rsx.at[i + 2, h], p_r.at[i + 2, h])
            for n in range(PART // 512):
                cols = pl.ds(n * 512, 512)
                rst[i, h, :, cols] = (part(h, cols) + rsx[i + 2, h, :, cols].astype(F32)).astype(BF)
            pass_on(i, h)
        return carry

    lax.fori_loop(0, NZ - 3, nearer, 0)

    part = combined(0)
    for h in range(2):
        landed(ret.at[0, h], e_r.at[0, h])
        landed(rsx.at[2, h], p_r.at[2, h])
        landed(rsx.at[1, h], p_r.at[1, h])
        for n in range(PART // 512):
            cols, wide = pl.ds(n * 512, 512), pl.ds(h * PART + n * 512, 512)
            routed = part(h, cols) + rsx[2, h, :, cols].astype(F32) + rsx[1, h, :, cols].astype(F32)
            out[:, wide] = (resid[:, wide].astype(F32) + sacc[:, wide] + routed).astype(BF)

    for i in range(NZ):
        landed(tx.at[i, :, pl.ds(0, PLANE - 1)], d_s.at[i])
        if i > 0:
            landed(info.at[i], i_s.at[i])
        for h in range(2):
            landed(rx.at[i, h, pl.ds(0, PLANE - 1)], e_s.at[i, h])
            if i > 0:
                landed(tok.at[i, h], z_s.at[i, h])
                landed(rst.at[i, h], p_s.at[i, h])
    landed(ekv.at[:, pl.ds(0, WINDOW)], h_s.at[0])
    landed(edoc.at[0], h_s.at[1])
    landed(ekv.at[:, pl.ds(0, WINDOW)], h_s.at[2])
    landed(edoc.at[0], h_s.at[3])
    landed(wo.at[others, direct], f_s.at[0])
    landed(wo.at[others, spread], f_s.at[1])
    for dx in range(1, NX):
        landed(atf.at[0], a_s.at[dx])
        landed(wo.at[0, direct], o_s.at[dx])
        landed(wo.at[0, share], g_s.at[0, dx])
        landed(wo.at[others, share], g_s.at[1, dx])
        landed(sg.at[0], x_s.at[0, dx])
        landed(su.at[0], x_s.at[1, dx])
        landed(sd.at[0], x_s.at[2, dx])


def shards(
    queries,
    keys,
    values,
    doc_ids,
    sink_logit,
    w_out,
    residual,
    ffn_gain,
    expert_ids,
    expert_weight,
    exp_gate,
    exp_up,
    exp_down,
    shared_gate,
    shared_up,
    shared_down,
):
    vmem = pl.BlockSpec(memory_space=pltpu.VMEM)
    smem = pl.BlockSpec(memory_space=pltpu.SMEM)
    hbm = pl.BlockSpec(memory_space=pl.ANY)
    dma = pltpu.SemaphoreType.DMA
    unit = FF // NX
    return pl.pallas_call(
        layer_kernel,
        out_shape=jax.ShapeDtypeStruct((ROWS, D), BF),
        in_specs=[hbm, vmem, vmem, vmem, smem, hbm, hbm, vmem, vmem, vmem] + [hbm] * 6,
        out_specs=vmem,
        scratch_shapes=[
            pltpu.VMEM((SPAN, HEADS * HD), BF),
            pltpu.VMEM((2 * HD, SPAN + 2 * WINDOW), BF),
            pltpu.VMEM((BLOCKS + 2, 8, ROWS), F32),
            pltpu.VMEM((BLOCKS, ROWS, HEADS * HD), BF),
            pltpu.VMEM((NX, ROWS, HEADS * HD), BF),
            pltpu.VMEM((NX, OUT_ROWS, D), BF),
            pltpu.VMEM((ROWS, D), BF),
            pltpu.VMEM((NZ, 2, ROWS, PART), BF),
            pltpu.VMEM((NZ, 2, PLANE, SLOTS, PART), BF),
            pltpu.VMEM((NZ, 2, PLANE, SLOTS, PART), BF),
            pltpu.VMEM((NZ, 2, PLANE, SLOTS, PART), BF),
            pltpu.VMEM((NZ, 2, ROWS, PART), BF),
            pltpu.VMEM((NZ, 2, ROWS, PART), BF),
            pltpu.VMEM((NZ, 2 * PLANE, ROWS), F32),
            pltpu.VMEM((NZ, 2 * PLANE, ROWS), F32),
            pltpu.VMEM((D, FF), BF),
            pltpu.VMEM((D, FF), BF),
            pltpu.VMEM((FF, D), BF),
            pltpu.VMEM((NX, D, unit), BF),
            pltpu.VMEM((NX, D, unit), BF),
            pltpu.VMEM((NX, unit, D), BF),
            pltpu.VMEM((ROWS, D), F32),
            pltpu.VMEM((PACK, FF), BF),
        ]
        + [dma((4,))] * 8
        + [dma((2, NX))] * 2
        + [dma((NZ, 2))] * 2
        + [dma((NZ,))] * 4
        + [dma((NZ, 2))] * 4
        + [dma((3, NX)), dma((3, NX)), dma((9,))],
        compiler_params=pltpu.CompilerParams(
            collective_id=1, has_side_effects=True, vmem_limit_bytes=62 * 2**20
        ),
        name="layer",
    )(
        queries, keys.T, values.T, doc_ids.reshape(BLOCKS, ROWS), sink_logit, w_out, residual,
        ffn_gain.reshape(1, D), expert_ids.T, expert_weight.T,
        exp_gate, exp_up, exp_down, shared_gate, shared_up, shared_down,
    )


def solution(mesh):
    placed = (
        P("sp", "tp"),
        P("sp", "tp"),
        P("sp", "tp"),
        P("sp"),
        P("tp"),
        P("tp", None),
        P(("sp", "tp"), None),
        P(),
        P(("sp", "tp"), None),
        P(("sp", "tp"), None),
        P("sp", None, None),
        P("sp", None, None),
        P("sp", None, None),
        P(None, "tp"),
        P(None, "tp"),
        P("tp", None),
    )
    return jax.shard_map(
        shards, mesh=mesh, in_specs=placed, out_specs=P(("sp", "tp"), None), check_vma=False
    )
```

time: 198 us -> 178 us (0.90)
  Pallas kernels: 193 us -> 176 us
  local copies, waits for them, and re-layouts: 5.07 us -> 1.88 us
    pallas_call x1, Pallas kernels: 193 us -> 176 us  [shards(): pl.pallas_call(layer_kernel, out_shape=jax.ShapeDtypeStruct((ROWS, D), BF...]
    unnamed x3 -> x1, local copies, waits for them, and re-layouts: 5.07 us -> 1.88 us
where the time goes in v3:
time: 178 us
  Pallas kernels  176 us (99%)
  local copies, waits for them, and re-layouts  1.88 us (1%)
    pallas_call x1, Pallas kernels, shards(): pl.pallas_call(layer_kernel, out_shape=jax.ShapeDtypeStruct((ROWS, D), BF...  176 us

profile of v3, /device:TPU:1, one launch (start us, length us, event | category | flops | bytes accessed | tf_op | source)
XLA Modules:
  0.0 178.2 jit_solution(12805874715575805670)
XLA Ops:
  0.0 176.3 %layer.1 = bf16[128,2048]{1,0:T(8,128)(2,1)} custom-call(bf16[512,256]{1,0:T(8,128)(2,1)} %q.1, bf16[64,512]{1,0:T(8,128)(2,1)} %bitcast.6, bf16[64,512]{1,0:T(8,128)(2,1)} %bitcast.7, s32[4,128]{1,0:T(4,128)} %bitcast.11, f32[4]{0:T(128)} %sink.1, bf16[256,2048]{1,0:T(8,128)(2,1)} %wout.1, bf16[128,2048]{1,0:T(8,128)(2,1)} %residual.1, f32[1,2048]{1,0:T(1,128)} %bitcast.8, ...), custom_call_target="tpu_custom_call" | custom-call | tf_op jit(solution)/shard_map/layer/pallas_call | solution.py:468
  176.4 1.9 %copy.18 = bf16[128,2048]{1,0:T(8,128)(2,1)} copy(bf16[128,2048]{1,0:T(8,128)(2,1)} %layer.1) | data formatting | bytes 1048576

commit v4 on v3

--- a/solution.py
+++ b/solution.py
@@ -17,8 +17,6 @@
 HEADS = 4
 OUT_ROWS = HEADS * HD
 OUT_HALF = OUT_ROWS // NC
-DIRECT = 64
-SHARE = (OUT_HALF - DIRECT) // NY
 PART = 1024
 ROWS = 128
 HALF = 64
@@ -47,12 +45,16 @@
     return 0 if delta == 0 else (2 * delta - 1 if delta <= NZ // 2 else 2 * (NZ - delta))
 
 
+NEAR = 6
+ROUTES = tuple((2 * n + turn, step, turn) for n, step in enumerate((0, 1, -1, 0)) for turn in range(NC))
+
+
 def layer_kernel(
     q, k, v, docs, sink, wout, residual, gain, ids, weight, eg, eu, ed, shg, shu, shd, out,
     qv, ekv, edoc, attn, atf, wo, resid,
-    tok, tx, rx, ret, rst, rsx, info, inf, wg, wu, wd, sg, su, sd, sacc, hid,
-    h_s, h_r, a_s, a_r, o_s, o_r, f_s, f_r, g_s, g_r,
-    z_s, z_r, i_s, i_r, d_s, d_r, e_s, e_r, p_s, p_r, x_s, x_r, w_s,
+    tok, tx, rx, ret, rst, rsx, info, inf, wg, wu, wd, vg, vu, vd, sg, su, sd, sacc, hid,
+    h_s, h_r, a_s, a_r, o_s, o_r, f_s, f_r,
+    z_s, z_r, i_s, i_r, d_s, d_r, e_s, e_r, p_s, p_r, x_s, x_r, t_s, t_r, q_s, q_r, u_s, u_r, w_s,
 ):
     sp, x = lax.axis_index("sp"), lax.axis_index("tp")
     z, mine = sp // PLANE, sp % PLANE
@@ -70,6 +72,9 @@
 
     def at_x(dx):
         return (sp, (x + dx) % NX)
+
+    def plane_of(dy, turn):
+        return (mine // NC + dy + NY) % NY * NC + (core + turn) % NC
 
     def send(src, dst, ssem, rsem, device):
         copy = pltpu.make_async_remote_copy(
@@ -106,18 +111,58 @@
     for b in range(BLOCKS):
         edoc[b + 1] = jnp.broadcast_to(docs[b : b + 1, :].astype(F32), (8, ROWS))
 
+    far = (vg, vu, vd)
+
+    def quarter(a, step):
+        rows = far[a].shape[0] // NX
+        return pl.ds(pl.multiple_of((x + step) % NX * rows, rows), rows)
+
+    def eighth(a, step, k):
+        rows = far[a].shape[0] // NX
+        return pl.ds(pl.multiple_of((x + step) % NX * rows + k * (rows // 2), rows // 2), rows // 2)
+
+    def unit(k):
+        return (0 if k == 3 else k, eighth(0, 0, k // 3) if k % 3 == 0 else quarter(k, 0))
+
+    def far_fetch(k):
+        a, rows = unit(k)
+        send((eg, eu, ed)[a].at[0, rows], far[a].at[rows], q_s.at[k], q_r.at[k], at_plane((mine + PLANE // 2) % PLANE))
+
+    def far_start(k):
+        a, rows = unit(k)
+        own = far[a].at[rows]
+        landed(own, q_r.at[k])
+        send(own, own, u_s.at[k, 1], u_r.at[k, 1], at_x(1))
+        send(own, own, u_s.at[k, 3], u_r.at[k, 3], at_x(3))
+
+    def far_relay(a):
+        if a == 0:
+            landed(far[0].at[eighth(0, 3, 0)], u_r.at[0, 1])
+            landed(far[0].at[eighth(0, 3, 1)], u_r.at[3, 1])
+        else:
+            landed(far[a].at[quarter(a, 3)], u_r.at[a, 1])
+        half = far[a].at[eighth(a, 3, 0)]
+        send(half, half, u_s.at[a, 0], u_r.at[a, 0], at_x(1))
+        if a == 0:
+            landed(far[0].at[eighth(0, 1, 0)], u_r.at[0, 3])
+            landed(far[0].at[eighth(0, 1, 1)], u_r.at[3, 3])
+        else:
+            landed(far[a].at[quarter(a, 1)], u_r.at[a, 3])
+        half = far[a].at[eighth(a, 1, 1)]
+        send(half, half, u_s.at[a, 2], u_r.at[a, 2], at_x(3))
+
+    def far_end(a):
+        landed(far[a].at[eighth(a, 2, 0)], u_r.at[a, 0])
+        landed(far[a].at[eighth(a, 2, 1)], u_r.at[a, 2])
+
     pl.semaphore_wait(barrier, len(peers))
     send(ekv.at[:, pl.ds(WINDOW, WINDOW)], ekv.at[:, pl.ds(WINDOW + SPAN, WINDOW)], h_s.at[0], h_r.at[0], at_sp(SP - 1))
     send(edoc.at[1], edoc.at[BLOCKS + 1], h_s.at[1], h_r.at[1], at_sp(SP - 1))
     send(ekv.at[:, pl.ds(SPAN, WINDOW)], ekv.at[:, pl.ds(0, WINDOW)], h_s.at[2], h_r.at[2], at_sp(1))
     send(edoc.at[BLOCKS], edoc.at[0], h_s.at[3], h_r.at[3], at_sp(1))
-    lower = core * OUT_HALF
-    direct = pl.ds(pl.multiple_of(lower, OUT_HALF), DIRECT)
-    spread = pl.ds(pl.multiple_of(lower + DIRECT, SHARE), OUT_HALF - DIRECT)
-    share = pl.ds(pl.multiple_of(lower + DIRECT + mine // NC * SHARE, SHARE), SHARE)
+    direct = pl.ds(pl.multiple_of(core * OUT_HALF, OUT_HALF), OUT_HALF)
+    rest = pl.ds(pl.multiple_of((1 - core) * OUT_HALF, OUT_HALF), OUT_HALF)
     others = pl.ds(1, NX - 1)
-    for dx in (1, 3, 2):
-        send(wout.at[share], wo.at[dx, share], g_s.at[0, dx], g_r.at[0, dx], at_x(dx))
     for dx in (1, 3, 2):
         send(wout.at[direct], wo.at[dx, direct], o_s.at[dx], o_r.at[dx], at_x(dx))
 
@@ -200,22 +245,19 @@
 
     for copy in local[2:]:
         copy.start()
-    for dx in (1, 3, 2):
-        landed(wo.at[dx, share], g_r.at[0, dx])
-    for dy in range(1, NY):
-        send(wo.at[others, share], wo.at[others, share], g_s.at[1, dy], g_r.at[1, dy], at_plane((mine + NC * dy) % PLANE))
+    for k in (0, 3, 1, 2):
+        far_fetch(k)
     for dx in (1, 3, 2):
         landed(wo.at[dx, direct], o_r.at[dx])
-    send(wo.at[others, direct], wo.at[others, direct], f_s.at[0], f_r.at[0], twin)
-    for dy in range(1, NY):
-        landed(wo.at[others, share], g_r.at[1, dy])
-    send(wo.at[others, spread], wo.at[others, spread], f_s.at[1], f_r.at[1], twin)
+        send(wo.at[dx, direct], wo.at[dx, direct], f_s.at[dx], f_r.at[dx], twin)
     local[1].wait()
     local[2].wait()
     for dx in range(NX):
         landed(atf.at[dx], a_r.at[dx])
-    landed(wo.at[others, direct], f_r.at[0])
-    landed(wo.at[others, spread], f_r.at[1])
+    for dx in range(1, NX):
+        landed(wo.at[dx, rest], f_r.at[dx])
+
+    far_start(0)
 
     def project(n, squares):
         cols = pl.ds(pl.multiple_of(n * 256, 256), 256)
@@ -245,110 +287,216 @@
         slot = lax.broadcasted_iota(jnp.int32, (PLANE, SLOTS, ROWS), 1).astype(F32)
         return (inf[i, 0:PLANE, :][:, None, :] == slot).astype(F32)
 
-    def dispatch(i, h):
-        @pl.when(i > 0)
-        def _():
-            landed(tok.at[i, h], z_r.at[i, h])
-
-            @pl.when(h == 0)
-            def _():
-                landed(inf.at[i], i_r.at[i])
-
-        @pl.when((i > 0) & (i + 2 < NZ))
+    def forward(i, h):
+        landed(tok.at[i, h], z_r.at[i, h])
+
+        @pl.when(h == 0)
+        def _():
+            landed(inf.at[i], i_r.at[i])
+
+        @pl.when((i < 5) | ((i == 5) & (h == 0)) | ((i == 6) & (h == 1)))
         def _():
             way = 1 + (NZ - 2) * ((i + 1) % 2)
-            send(tok.at[i, h], tok.at[i + 2, h], z_s.at[i + 2, h], z_r.at[i + 2, h], at_z(way))
-
+            to = jnp.minimum(i + 2, NZ - 1)
+            send(tok.at[i, h], tok.at[to, h], z_s.at[to, h], z_r.at[to, h], at_z(way))
+
+    def pack(i, h):
         pick = placed(i).reshape(PACK, ROWS).astype(BF)
         for n in range(PART // 512):
             cols = pl.ds(n * 512, 512)
             tx[i, h, :, :, cols] = dot(pick, tok[i, h, :, cols]).astype(BF).reshape(PLANE, SLOTS, 512)
-        for off in range(1, PLANE):
-            j = (mine + off) % PLANE
-            send(tx.at[i, h, j], rx.at[i, h, mine], d_s.at[i], d_r.at[i], at_plane(j))
-        pltpu.make_async_copy(tx.at[i, h, mine], rx.at[i, h, mine], d_r.at[i]).start()
-
-    def run_expert(i):
-        landed(rx.at[i], d_r.at[i])
+        for slot, step, turn in ROUTES:
+            runner = plane_of(-step, turn)
+            expert = plane_of(2, turn) if slot >= NEAR else runner
+            if step == 0 and turn == 0:
+                pltpu.make_async_copy(tx.at[i, h, expert], rx.at[i, h, slot], d_r.at[i]).start()
+            else:
+                send(tx.at[i, h, expert], rx.at[i, h, slot], d_s.at[i], d_r.at[i], at_plane(runner))
+
+    def run_expert(i, lower, count, gate_w, up_w, down_w):
+        rows, slots = count * SLOTS, pl.ds(lower, count)
 
         def hidden_tile(n, carry):
             cols = pl.ds(pl.multiple_of(n * 256, 256), 256)
-            left, right = rx[i, 0].reshape(PACK, PART), rx[i, 1].reshape(PACK, PART)
-            gate = dot(left, wg[0:PART, cols]) + dot(right, wg[PART:D, cols])
-            up = dot(left, wu[0:PART, cols]) + dot(right, wu[PART:D, cols])
-            hid[:, cols] = (silu(gate) * up).astype(BF)
+            left, right = rx[i, 0, slots].reshape(rows, PART), rx[i, 1, slots].reshape(rows, PART)
+            gate = dot(left, gate_w[0:PART, cols]) + dot(right, gate_w[PART:D, cols])
+            up = dot(left, up_w[0:PART, cols]) + dot(right, up_w[PART:D, cols])
+            hid[0:rows, cols] = (silu(gate) * up).astype(BF)
             return carry
 
         lax.fori_loop(0, FF // 256, hidden_tile, 0)
 
         def out_tile(n, carry):
             cols = pl.ds(pl.multiple_of(n * 512, 512), 512)
-            made = dot(hid[...], wd[:, cols]).astype(BF).reshape(PLANE, SLOTS, 512)
-            rx[i, n // 2, :, :, pl.ds(pl.multiple_of(n % 2 * 512, 512), 512)] = made
+            made = dot(hid[0:rows, :], down_w[:, cols]).astype(BF).reshape(count, SLOTS, 512)
+            rx[i, n // 2, slots, :, pl.ds(pl.multiple_of(n % 2 * 512, 512), 512)] = made
             return carry
 
         lax.fori_loop(0, D // 512, out_tile, 0)
 
-    def give_back(i):
+    def give_back(i, routes):
         for h in range(2):
-            for off in range(1, PLANE):
-                j = (mine + off) % PLANE
-                send(rx.at[i, h, j], ret.at[i, h, mine], e_s.at[i, h], e_r.at[i, h], at_plane(j))
-            pltpu.make_async_copy(rx.at[i, h, mine], ret.at[i, h, mine], e_r.at[i, h]).start()
+            for slot, step, turn in routes:
+                source = plane_of(step, turn)
+                expert = plane_of(2, 0) if slot >= NEAR else mine
+                if step == 0 and turn == 0:
+                    pltpu.make_async_copy(rx.at[i, h, slot], ret.at[i, h, expert], e_r.at[i, h]).start()
+                else:
+                    send(rx.at[i, h, slot], ret.at[i, h, expert], e_s.at[i, h], e_r.at[i, h], at_plane(source))
+
+    def run_near(i):
+        landed(rx.at[i], d_r.at[i])
+        run_expert(i, 0, NEAR, wg, wu, wd)
+
+    def run_far(i):
+        run_expert(i, NEAR, PLANE - NEAR, vg, vu, vd)
+        give_back(i, ROUTES[NEAR:])
 
     def pieces(n, carry):
-        m = jnp.maximum(n - 2, 0)
-        i = jnp.where(n < 2, 0, 1 + m // 4 * 2 + m % 2)
-        h = jnp.where(n < 2, n, m % 4 // 2)
+        i = 1 + n // 4 * 2 + n % 2
+        h = n % 4 // 2
 
         @pl.when(i < NZ)
         def _():
-            dispatch(i, h)
-
-        @pl.when(n == 1)
-        def _():
-            for copy in local[3:6]:
-                copy.wait()
-            for dx in range(1, NX):
-                send(sg.at[0], sg.at[dx], x_s.at[0, dx], x_r.at[0, dx], at_x(dx))
-                send(su.at[0], su.at[dx], x_s.at[1, dx], x_r.at[1, dx], at_x(dx))
-                send(sd.at[0], sd.at[dx], x_s.at[2, dx], x_r.at[2, dx], at_x(dx))
-            for copy in local[6:]:
-                copy.wait()
-
-        @pl.when((n == 9) | (n == 13))
-        def _():
-            def early(j, carry):
-                run_expert((n - 9) // 2 + j)
-                return carry
-
-            lax.fori_loop(0, 2, early, 0)
+            forward(i, h)
+
+            @pl.when(i >= 3)
+            def _():
+                pack(i, h)
+
+        for at, task in (
+            (1, lambda: far_start(2)),
+            (3, lambda: far_relay(0)),
+            (7, lambda: far_relay(1)),
+            (11, lambda: far_relay(2)),
+            (12, shared_start),
+        ):
+            pl.when(n == at)(task)
+
+        @pl.when((n == 9) | (n == 11))
+        def _():
+            run_near((n - 3) // 2)
 
         return carry
 
-    lax.fori_loop(0, 2 + 2 * NZ, pieces, 0)
-
-    def late(j, carry):
-        run_expert(j)
-
-        @pl.when(j >= NZ - 2)
-        def _():
-            give_back(j)
+    shared = ((shg, sg), (shu, su), (shd, sd))
+
+    def twin_half(a, which):
+        rows = shared[a][0].shape[0] // NC
+        return pl.ds(pl.multiple_of(which * rows, rows), rows)
+
+    def shared_start():
+        for copy in local[3:6]:
+            copy.wait()
+        for dx in (1, 3, 2):
+            for a, (mat, full) in enumerate(shared):
+                rows = twin_half(a, core)
+                send(full.at[0, rows], full.at[dx, rows], x_s.at[a, dx], x_r.at[a, dx], at_x(dx))
+
+    def shared_relay():
+        for a, (_, full) in enumerate(shared):
+            rows = twin_half(a, core)
+            for dx in (1, 3, 2):
+                landed(full.at[dx, rows], x_r.at[a, dx])
+            send(full.at[others, rows], full.at[others, rows], t_s.at[a], t_r.at[a], twin)
+
+    far_start(3)
+    far_start(1)
+    for copy in local[6:]:
+        copy.wait()
+    lax.fori_loop(0, 2 * NZ - 1, pieces, 0)
+
+    near_routes = ROUTES[:NEAR]
+    run_near(5)
+    run_near(6)
+    give_back(6, near_routes)
+    run_near(7)
+    give_back(7, near_routes)
+    give_back(5, near_routes)
+    for a in range(3):
+        far_end(a)
+    run_far(7)
+
+    def nearest(n, carry):
+        pack((n // 2 + 1) % 3, n % 2)
+
+        @pl.when(n == 3)
+        def _():
+            give_back(4, near_routes)
+            give_back(3, near_routes)
 
         return carry
 
-    lax.fori_loop(4, NZ, late, 0)
-
-    def backward(n, carry):
-        give_back(NZ - 3 - n)
+    lax.fori_loop(0, 6, nearest, 0)
+    run_far(6)
+
+    def combined(i):
+        scaled = placed(i) * inf[i, PLANE : 2 * PLANE, :][:, None, :]
+        scaled = jnp.concatenate([scaled.reshape(PACK, ROWS), jnp.zeros((256 - PACK, ROWS), F32)], axis=0)
+        scaled = scaled.T[:, :PACK]
+        high = scaled.astype(BF)
+        low = (scaled - high.astype(F32)).astype(BF)
+
+        def part(h, cols):
+            rows = ret[i, h, :, :, cols].reshape(PACK, 512)
+            return dot(high, rows) + dot(low, rows)
+
+        return part
+
+    def pass_on(i, h, way):
+        send(rst.at[i, h], rsx.at[i, h], p_s.at[i, h], p_r.at[i, h], at_z(way))
+
+    def reduce_chunk(i, ways, arrives):
+        part = combined(i)
+        for h in range(2):
+            landed(ret.at[i, h], e_r.at[i, h])
+            source = arrives[h]
+            if source is not None:
+                landed(rsx.at[source, h], p_r.at[source, h])
+            for n in range(PART // 512):
+                cols = pl.ds(n * 512, 512)
+                total = part(h, cols)
+                if source is not None:
+                    total = total + rsx[source, h, :, cols].astype(F32)
+                rst[i, h, :, cols] = total.astype(BF)
+            pass_on(i, h, ways[h])
+
+    reduce_chunk(7, (NZ - 1, 1), (None, None))
+    run_far(5)
+    reduce_chunk(6, (1, 1), (None, 7))
+    reduce_chunk(5, (NZ - 1, NZ - 1), (7, None))
+
+    def middle(n, carry):
+        run_far(4 - n)
+        run_near(2 - n)
+        give_back(2 - n, near_routes)
         return carry
 
-    lax.fori_loop(0, NZ - 2, backward, 0)
-
-    for dx in range(1, NX):
-        landed(sg.at[dx], x_r.at[0, dx])
-        landed(su.at[dx], x_r.at[1, dx])
-        landed(sd.at[dx], x_r.at[2, dx])
+    lax.fori_loop(0, 2, middle, 0)
+
+    def nearer(n, carry):
+        i = 4 - n
+        way = 1 + (NZ - 2) * (i % 2)
+
+        @pl.when(n == 2)
+        def _():
+            run_near(0)
+            give_back(0, near_routes)
+            run_far(2)
+
+        reduce_chunk(i, (way, way), (i + 2, i + 2))
+
+        @pl.when(n >= 2)
+        def _():
+            run_far(3 - n)
+
+        pl.when(n == 2)(shared_relay)
+        return carry
+
+    lax.fori_loop(0, 4, nearer, 0)
+
+    for a, (_, full) in enumerate(shared):
+        landed(full.at[others, twin_half(a, 1 - core)], t_r.at[a])
     sacc[...] = jnp.zeros_like(sacc)
 
     def shared_block(dx, carry):
@@ -363,50 +511,6 @@
 
     lax.fori_loop(0, NX, shared_block, 0)
 
-    def combined(i):
-        scaled = placed(i) * inf[i, PLANE : 2 * PLANE, :][:, None, :]
-        scaled = jnp.concatenate([scaled.reshape(PACK, ROWS), jnp.zeros((256 - PACK, ROWS), F32)], axis=0)
-        scaled = scaled.T[:, :PACK]
-        high = scaled.astype(BF)
-        low = (scaled - high.astype(F32)).astype(BF)
-
-        def part(h, cols):
-            rows = ret[i, h, :, :, cols].reshape(PACK, 512)
-            return dot(high, rows) + dot(low, rows)
-
-        return part
-
-    def pass_on(i, h):
-        way = NZ - 1 - (NZ - 2) * ((i + 1) % 2)
-        send(rst.at[i, h], rsx.at[i, h], p_s.at[i, h], p_r.at[i, h], at_z(way))
-
-    def farthest(n, carry):
-        i = NZ - 2 + n
-        part = combined(i)
-        for h in range(2):
-            landed(ret.at[i, h], e_r.at[i, h])
-            for n in range(PART // 512):
-                cols = pl.ds(n * 512, 512)
-                rst[i, h, :, cols] = part(h, cols).astype(BF)
-            pass_on(i, h)
-        return carry
-
-    lax.fori_loop(0, 2, farthest, 0)
-
-    def nearer(n, carry):
-        i = NZ - 3 - n
-        part = combined(i)
-        for h in range(2):
-            landed(ret.at[i, h], e_r.at[i, h])
-            landed(rsx.at[i + 2, h], p_r.at[i + 2, h])
-            for n in range(PART // 512):
-                cols = pl.ds(n * 512, 512)
-                rst[i, h, :, cols] = (part(h, cols) + rsx[i + 2, h, :, cols].astype(F32)).astype(BF)
-            pass_on(i, h)
-        return carry
-
-    lax.fori_loop(0, NZ - 3, nearer, 0)
-
     part = combined(0)
     for h in range(2):
         landed(ret.at[0, h], e_r.at[0, h])
@@ -418,11 +522,11 @@
             out[:, wide] = (resid[:, wide].astype(F32) + sacc[:, wide] + routed).astype(BF)
 
     for i in range(NZ):
-        landed(tx.at[i, :, pl.ds(0, PLANE - 1)], d_s.at[i])
+        landed(tx.at[i, :, pl.ds(0, PLANE - 2)], d_s.at[i])
         if i > 0:
             landed(info.at[i], i_s.at[i])
         for h in range(2):
-            landed(rx.at[i, h, pl.ds(0, PLANE - 1)], e_s.at[i, h])
+            landed(rx.at[i, h, pl.ds(0, PLANE - 2)], e_s.at[i, h])
             if i > 0:
                 landed(tok.at[i, h], z_s.at[i, h])
                 landed(rst.at[i, h], p_s.at[i, h])
@@ -430,16 +534,21 @@
     landed(edoc.at[0], h_s.at[1])
     landed(ekv.at[:, pl.ds(0, WINDOW)], h_s.at[2])
     landed(edoc.at[0], h_s.at[3])
-    landed(wo.at[others, direct], f_s.at[0])
-    landed(wo.at[others, spread], f_s.at[1])
     for dx in range(1, NX):
         landed(atf.at[0], a_s.at[dx])
         landed(wo.at[0, direct], o_s.at[dx])
-        landed(wo.at[0, share], g_s.at[0, dx])
-        landed(wo.at[others, share], g_s.at[1, dx])
-        landed(sg.at[0], x_s.at[0, dx])
-        landed(su.at[0], x_s.at[1, dx])
-        landed(sd.at[0], x_s.at[2, dx])
+        landed(wo.at[0, direct], f_s.at[dx])
+        for a, (_, full) in enumerate(shared):
+            landed(full.at[0, twin_half(a, core)], x_s.at[a, dx])
+    for a, (_, full) in enumerate(shared):
+        landed(full.at[others, twin_half(a, core)], t_s.at[a])
+        landed(far[a].at[eighth(a, 0, 0)], u_s.at[a, 0])
+        landed(far[a].at[eighth(a, 0, 0)], u_s.at[a, 2])
+    for k in range(4):
+        a, rows = unit(k)
+        landed(far[a].at[rows], q_s.at[k])
+        landed(far[a].at[rows], u_s.at[k, 1])
+        landed(far[a].at[rows], u_s.at[k, 3])
 
 
 def shards(
@@ -489,6 +598,9 @@
             pltpu.VMEM((D, FF), BF),
             pltpu.VMEM((D, FF), BF),
             pltpu.VMEM((FF, D), BF),
+            pltpu.VMEM((D, FF), BF),
+            pltpu.VMEM((D, FF), BF),
+            pltpu.VMEM((FF, D), BF),
             pltpu.VMEM((NX, D, unit), BF),
             pltpu.VMEM((NX, D, unit), BF),
             pltpu.VMEM((NX, unit, D), BF),
@@ -496,11 +608,14 @@
             pltpu.VMEM((PACK, FF), BF),
         ]
         + [dma((4,))] * 8
-        + [dma((2, NX))] * 2
         + [dma((NZ, 2))] * 2
         + [dma((NZ,))] * 4
         + [dma((NZ, 2))] * 4
-        + [dma((3, NX)), dma((3, NX)), dma((9,))],
+        + [dma((3, NX))] * 2
+        + [dma((3,))] * 2
+        + [dma((4,))] * 2
+        + [dma((4, NX))] * 2
+        + [dma((9,))],
         compiler_params=pltpu.CompilerParams(
             collective_id=1, has_side_effects=True, vmem_limit_bytes=62 * 2**20
         ),

time: 178 us -> 156 us (0.88)
  Pallas kernels: 176 us -> 154 us
    pallas_call x1, Pallas kernels: 176 us -> 154 us  [shards(): pl.pallas_call(layer_kernel, out_shape=jax.ShapeDtypeStruct((ROWS, D), BF...]
where the time goes in v4:
time: 156 us
  Pallas kernels  154 us (99%)
  local copies, waits for them, and re-layouts  1.88 us (1%)
    pallas_call x1, Pallas kernels, shards(): pl.pallas_call(layer_kernel, out_shape=jax.ShapeDtypeStruct((ROWS, D), BF...  154 us

profile of v4, /device:TPU:1, one launch (start us, length us, event | category | flops | bytes accessed | tf_op | source)
XLA Modules:
  0.0 155.7 jit_solution(15583200941956094343)
XLA Ops:
  0.0 153.8 %layer.1 = bf16[128,2048]{1,0:T(8,128)(2,1)} custom-call(bf16[512,256]{1,0:T(8,128)(2,1)} %q.1, bf16[64,512]{1,0:T(8,128)(2,1)} %bitcast.6, bf16[64,512]{1,0:T(8,128)(2,1)} %bitcast.7, s32[4,128]{1,0:T(4,128)} %bitcast.11, f32[4]{0:T(128)} %sink.1, bf16[256,2048]{1,0:T(8,128)(2,1)} %wout.1, bf16[128,2048]{1,0:T(8,128)(2,1)} %residual.1, f32[1,2048]{1,0:T(1,128)} %bitcast.8, ...), custom_call_target="tpu_custom_call" | custom-call | tf_op jit(solution)/shard_map/layer/pallas_call | solution.py:577
  153.8 1.9 %copy.18 = bf16[128,2048]{1,0:T(8,128)(2,1)} copy(bf16[128,2048]{1,0:T(8,128)(2,1)} %layer.1) | data formatting | bytes 1048576

commit v5 on v4

--- a/solution.py
+++ b/solution.py
@@ -334,8 +334,8 @@
 
         lax.fori_loop(0, D // 512, out_tile, 0)
 
-    def give_back(i, routes):
-        for h in range(2):
+    def give_back(i, routes, halves=(0, 1)):
+        for h in halves:
             for slot, step, turn in routes:
                 source = plane_of(step, turn)
                 expert = plane_of(2, 0) if slot >= NEAR else mine
@@ -359,10 +359,7 @@
         @pl.when(i < NZ)
         def _():
             forward(i, h)
-
-            @pl.when(i >= 3)
-            def _():
-                pack(i, h)
+            pack(i, h)
 
         for at, task in (
             (1, lambda: far_start(2)),
@@ -373,9 +370,9 @@
         ):
             pl.when(n == at)(task)
 
-        @pl.when((n == 9) | (n == 11))
+        @pl.when((n >= 4) & (n != 6) & (n != 8) & (n < 12) & (n != 10))
         def _():
-            run_near((n - 3) // 2)
+            run_near(jnp.where(n < 6, n - 4, (n - 3) // 2))
 
         return carry
 
@@ -400,6 +397,8 @@
                 landed(full.at[dx, rows], x_r.at[a, dx])
             send(full.at[others, rows], full.at[others, rows], t_s.at[a], t_r.at[a], twin)
 
+    pack(0, 0)
+    pack(0, 1)
     far_start(3)
     far_start(1)
     for copy in local[6:]:
@@ -409,26 +408,19 @@
     near_routes = ROUTES[:NEAR]
     run_near(5)
     run_near(6)
-    give_back(6, near_routes)
+    give_back(6, near_routes, (0,))
     run_near(7)
     give_back(7, near_routes)
-    give_back(5, near_routes)
+    give_back(6, near_routes, (1,))
     for a in range(3):
         far_end(a)
     run_far(7)
 
-    def nearest(n, carry):
-        pack((n // 2 + 1) % 3, n % 2)
-
-        @pl.when(n == 3)
-        def _():
-            give_back(4, near_routes)
-            give_back(3, near_routes)
-
+    def backward(n, carry):
+        give_back(5 - n, near_routes)
         return carry
 
-    lax.fori_loop(0, 6, nearest, 0)
-    run_far(6)
+    lax.fori_loop(0, 6, backward, 0)
 
     def combined(i):
         scaled = placed(i) * inf[i, PLANE : 2 * PLANE, :][:, None, :]
@@ -446,54 +438,41 @@
     def pass_on(i, h, way):
         send(rst.at[i, h], rsx.at[i, h], p_s.at[i, h], p_r.at[i, h], at_z(way))
 
-    def reduce_chunk(i, ways, arrives):
+    def reduce_piece(i, h, way, source=None):
         part = combined(i)
-        for h in range(2):
-            landed(ret.at[i, h], e_r.at[i, h])
-            source = arrives[h]
+        landed(ret.at[i, h], e_r.at[i, h])
+        if source is not None:
+            landed(rsx.at[source, h], p_r.at[source, h])
+        for n in range(PART // 512):
+            cols = pl.ds(n * 512, 512)
+            total = part(h, cols)
             if source is not None:
-                landed(rsx.at[source, h], p_r.at[source, h])
-            for n in range(PART // 512):
-                cols = pl.ds(n * 512, 512)
-                total = part(h, cols)
-                if source is not None:
-                    total = total + rsx[source, h, :, cols].astype(F32)
-                rst[i, h, :, cols] = total.astype(BF)
-            pass_on(i, h, ways[h])
-
-    reduce_chunk(7, (NZ - 1, 1), (None, None))
+                total = total + rsx[source, h, :, cols].astype(F32)
+            rst[i, h, :, cols] = total.astype(BF)
+        pass_on(i, h, way)
+
+    reduce_piece(7, 0, NZ - 1)
+    reduce_piece(7, 1, 1)
+    run_far(6)
+    reduce_piece(6, 0, 1)
     run_far(5)
-    reduce_chunk(6, (1, 1), (None, 7))
-    reduce_chunk(5, (NZ - 1, NZ - 1), (7, None))
-
-    def middle(n, carry):
-        run_far(4 - n)
-        run_near(2 - n)
-        give_back(2 - n, near_routes)
+    reduce_piece(5, 1, NZ - 1)
+    reduce_piece(5, 0, NZ - 1, 7)
+    reduce_piece(6, 1, 1, 7)
+
+    def nearer(n, carry):
+        even, odd = 4 - 2 * n, 3 - 2 * n
+        run_far(even)
+        reduce_piece(even, 0, 1, even + 2)
+        run_far(odd)
+        reduce_piece(odd, 1, NZ - 1, odd + 2)
+        reduce_piece(even, 1, 1, even + 2)
+        reduce_piece(odd, 0, NZ - 1, odd + 2)
+        pl.when(n == 1)(shared_relay)
         return carry
 
-    lax.fori_loop(0, 2, middle, 0)
-
-    def nearer(n, carry):
-        i = 4 - n
-        way = 1 + (NZ - 2) * (i % 2)
-
-        @pl.when(n == 2)
-        def _():
-            run_near(0)
-            give_back(0, near_routes)
-            run_far(2)
-
-        reduce_chunk(i, (way, way), (i + 2, i + 2))
-
-        @pl.when(n >= 2)
-        def _():
-            run_far(3 - n)
-
-        pl.when(n == 2)(shared_relay)
-        return carry
-
-    lax.fori_loop(0, 4, nearer, 0)
+    lax.fori_loop(0, 2, nearer, 0)
+    run_far(0)
 
     for a, (_, full) in enumerate(shared):
         landed(full.at[others, twin_half(a, 1 - core)], t_r.at[a])

time: 156 us -> 148 us (0.949)
  Pallas kernels: 154 us -> 146 us
    pallas_call x1, Pallas kernels: 154 us -> 146 us  [shards(): pl.pallas_call(layer_kernel, out_shape=jax.ShapeDtypeStruct((ROWS, D), BF...]
where the time goes in v5:
time: 148 us
  Pallas kernels  146 us (99%)
  local copies, waits for them, and re-layouts  1.88 us (1%)
    pallas_call x1, Pallas kernels, shards(): pl.pallas_call(layer_kernel, out_shape=jax.ShapeDtypeStruct((ROWS, D), BF...  146 us

profile of v5, /device:TPU:1, one launch (start us, length us, event | category | flops | bytes accessed | tf_op | source)
XLA Modules:
  0.0 148.2 jit_solution(9462390893110291751)
XLA Ops:
  0.0 146.3 %layer.1 = bf16[128,2048]{1,0:T(8,128)(2,1)} custom-call(bf16[512,256]{1,0:T(8,128)(2,1)} %q.1, bf16[64,512]{1,0:T(8,128)(2,1)} %bitcast.6, bf16[64,512]{1,0:T(8,128)(2,1)} %bitcast.7, s32[4,128]{1,0:T(4,128)} %bitcast.11, f32[4]{0:T(128)} %sink.1, bf16[256,2048]{1,0:T(8,128)(2,1)} %wout.1, bf16[128,2048]{1,0:T(8,128)(2,1)} %residual.1, f32[1,2048]{1,0:T(1,128)} %bitcast.8, ...), custom_call_target="tpu_custom_call" | custom-call | tf_op jit(solution)/shard_map/layer/pallas_call | solution.py:556
  146.3 1.9 %copy.18 = bf16[128,2048]{1,0:T(8,128)(2,1)} copy(bf16[128,2048]{1,0:T(8,128)(2,1)} %layer.1) | data formatting | bytes 1048576

commit v6 on v5

--- a/solution.py
+++ b/solution.py
@@ -17,6 +17,7 @@
 HEADS = 4
 OUT_ROWS = HEADS * HD
 OUT_HALF = OUT_ROWS // NC
+DIRECT = 80
 PART = 1024
 ROWS = 128
 HALF = 64
@@ -53,7 +54,7 @@
     q, k, v, docs, sink, wout, residual, gain, ids, weight, eg, eu, ed, shg, shu, shd, out,
     qv, ekv, edoc, attn, atf, wo, resid,
     tok, tx, rx, ret, rst, rsx, info, inf, wg, wu, wd, vg, vu, vd, sg, su, sd, sacc, hid,
-    h_s, h_r, a_s, a_r, o_s, o_r, f_s, f_r,
+    h_s, h_r, a_s, a_r, o_s, o_r, f_s, f_r, g_s, g_r, c_s, c_r,
     z_s, z_r, i_s, i_r, d_s, d_r, e_s, e_r, p_s, p_r, x_s, x_r, t_s, t_r, q_s, q_r, u_s, u_r, w_s,
 ):
     sp, x = lax.axis_index("sp"), lax.axis_index("tp")
@@ -160,9 +161,17 @@
     send(edoc.at[1], edoc.at[BLOCKS + 1], h_s.at[1], h_r.at[1], at_sp(SP - 1))
     send(ekv.at[:, pl.ds(SPAN, WINDOW)], ekv.at[:, pl.ds(0, WINDOW)], h_s.at[2], h_r.at[2], at_sp(1))
     send(edoc.at[BLOCKS], edoc.at[0], h_s.at[3], h_r.at[3], at_sp(1))
-    direct = pl.ds(pl.multiple_of(core * OUT_HALF, OUT_HALF), OUT_HALF)
-    rest = pl.ds(pl.multiple_of((1 - core) * OUT_HALF, OUT_HALF), OUT_HALF)
+    def out_rows(which, start, size):
+        return pl.ds(pl.multiple_of(which * OUT_HALF + start, 16), size)
+
+    def share_cols(dz):
+        return pl.ds(pl.multiple_of((z + dz) % NZ * (D // NZ), D // NZ), D // NZ)
+
+    direct, spread = out_rows(core, 0, DIRECT), out_rows(core, DIRECT, OUT_HALF - DIRECT)
+    rest, rest_spread = out_rows(1 - core, 0, DIRECT), out_rows(1 - core, DIRECT, OUT_HALF - DIRECT)
     others = pl.ds(1, NX - 1)
+    for dx in (1, 3, 2):
+        send(wout.at[spread, share_cols(0)], wo.at[dx, spread, share_cols(0)], g_s.at[dx], g_r.at[dx], at_x(dx))
     for dx in (1, 3, 2):
         send(wout.at[direct], wo.at[dx, direct], o_s.at[dx], o_r.at[dx], at_x(dx))
 
@@ -194,6 +203,13 @@
             landed(edoc.at[BLOCKS + 1], h_r.at[1])
             landed(ekv.at[:, pl.ds(0, WINDOW)], h_r.at[2])
             landed(edoc.at[0], h_r.at[3])
+            for k in (0, 3, 1, 2):
+                far_fetch(k)
+            for dx in (1, 3, 2):
+                landed(wo.at[dx, spread, share_cols(0)], g_r.at[dx])
+            mine_of = wo.at[others, spread, share_cols(0)]
+            for dz in range(1, NZ):
+                send(mine_of, mine_of, c_s.at[dz], c_r.at[dz], at_z(dz))
 
             @pl.when(sp == 0)
             def _():
@@ -245,17 +261,19 @@
 
     for copy in local[2:]:
         copy.start()
-    for k in (0, 3, 1, 2):
-        far_fetch(k)
     for dx in (1, 3, 2):
         landed(wo.at[dx, direct], o_r.at[dx])
         send(wo.at[dx, direct], wo.at[dx, direct], f_s.at[dx], f_r.at[dx], twin)
+    for dz in range(1, NZ):
+        landed(wo.at[others, spread, share_cols(NZ - dz)], c_r.at[dz])
+    send(wo.at[others, spread], wo.at[others, spread], f_s.at[0], f_r.at[0], twin)
     local[1].wait()
     local[2].wait()
     for dx in range(NX):
         landed(atf.at[dx], a_r.at[dx])
     for dx in range(1, NX):
         landed(wo.at[dx, rest], f_r.at[dx])
+    landed(wo.at[others, rest_spread], f_r.at[0])
 
     far_start(0)
 
@@ -362,17 +380,18 @@
             pack(i, h)
 
         for at, task in (
-            (1, lambda: far_start(2)),
+            (1, lambda: far_start(1)),
             (3, lambda: far_relay(0)),
-            (7, lambda: far_relay(1)),
-            (11, lambda: far_relay(2)),
+            (5, lambda: far_start(2)),
+            (8, lambda: far_relay(1)),
+            (12, lambda: far_relay(2)),
             (12, shared_start),
         ):
             pl.when(n == at)(task)
 
-        @pl.when((n >= 4) & (n != 6) & (n != 8) & (n < 12) & (n != 10))
+        @pl.when((n == 6) | (n == 8) | (n == 10) | (n == 11))
         def _():
-            run_near(jnp.where(n < 6, n - 4, (n - 3) // 2))
+            run_near(jnp.where(n == 11, 3, (n - 6) // 2))
 
         return carry
 
@@ -400,12 +419,12 @@
     pack(0, 0)
     pack(0, 1)
     far_start(3)
-    far_start(1)
     for copy in local[6:]:
         copy.wait()
     lax.fori_loop(0, 2 * NZ - 1, pieces, 0)
 
     near_routes = ROUTES[:NEAR]
+    run_near(4)
     run_near(5)
     run_near(6)
     give_back(6, near_routes, (0,))
@@ -517,12 +536,16 @@
         landed(atf.at[0], a_s.at[dx])
         landed(wo.at[0, direct], o_s.at[dx])
         landed(wo.at[0, direct], f_s.at[dx])
+        landed(wo.at[0, spread, share_cols(0)], g_s.at[dx])
         for a, (_, full) in enumerate(shared):
             landed(full.at[0, twin_half(a, core)], x_s.at[a, dx])
     for a, (_, full) in enumerate(shared):
         landed(full.at[others, twin_half(a, core)], t_s.at[a])
         landed(far[a].at[eighth(a, 0, 0)], u_s.at[a, 0])
         landed(far[a].at[eighth(a, 0, 0)], u_s.at[a, 2])
+    landed(wo.at[others, spread], f_s.at[0])
+    for dz in range(1, NZ):
+        landed(wo.at[others, spread, share_cols(0)], c_s.at[dz])
     for k in range(4):
         a, rows = unit(k)
         landed(far[a].at[rows], q_s.at[k])
@@ -586,7 +609,8 @@
             pltpu.VMEM((ROWS, D), F32),
             pltpu.VMEM((PACK, FF), BF),
         ]
-        + [dma((4,))] * 8
+        + [dma((4,))] * 10
+        + [dma((NZ,))] * 2
         + [dma((NZ, 2))] * 2
         + [dma((NZ,))] * 4
         + [dma((NZ, 2))] * 4

time: 148 us -> 145 us (0.980)
  Pallas kernels: 146 us -> 143 us
    pallas_call x1, Pallas kernels: 146 us -> 143 us  [shards(): pl.pallas_call(layer_kernel, out_shape=jax.ShapeDtypeStruct((ROWS, D), BF...]
where the time goes in v6:
time: 145 us
  Pallas kernels  143 us (99%)
  local copies, waits for them, and re-layouts  1.88 us (1%)
    pallas_call x1, Pallas kernels, shards(): pl.pallas_call(layer_kernel, out_shape=jax.ShapeDtypeStruct((ROWS, D), BF...  143 us

profile of v6, /device:TPU:1, one launch (start us, length us, event | category | flops | bytes accessed | tf_op | source)
XLA Modules:
  0.0 144.7 jit_solution(17557378873277087306)
XLA Ops:
  0.0 142.8 %layer.1 = bf16[128,2048]{1,0:T(8,128)(2,1)} custom-call(bf16[512,256]{1,0:T(8,128)(2,1)} %q.1, bf16[64,512]{1,0:T(8,128)(2,1)} %bitcast.6, bf16[64,512]{1,0:T(8,128)(2,1)} %bitcast.7, s32[4,128]{1,0:T(4,128)} %bitcast.11, f32[4]{0:T(128)} %sink.1, bf16[256,2048]{1,0:T(8,128)(2,1)} %wout.1, bf16[128,2048]{1,0:T(8,128)(2,1)} %residual.1, f32[1,2048]{1,0:T(1,128)} %bitcast.8, ...), custom_call_target="tpu_custom_call" | custom-call | tf_op jit(solution)/shard_map/layer/pallas_call | solution.py:579
  142.8 1.9 %copy.18 = bf16[128,2048]{1,0:T(8,128)(2,1)} copy(bf16[128,2048]{1,0:T(8,128)(2,1)} %layer.1) | data formatting | bytes 1048576
